TPU v7x, 512 devices: a whole 4x8x8 slice. The times are simulated.
512 devices in a mesh: ep: 32 (over z, x), tp: 16 (over y, core).
Axes of the slice: x: 4, y: 8, z: 8, core: 2. Of those that a mesh axis runs over, the one named last changes fastest.
Arguments:
- tokens: bfloat16 [256, 2048], P('ep', 'tp'), may hold values from -10 to 10, as said below
- norm_gain: float32 [2048], P('tp'), may hold values from 0.5 to 1.5
- norm_bias: float32 [2048], P('tp'), may hold values from -0.3 to 0.3
- group_pick: int32 [256, 1], P('ep'), may hold values from 0 to 7; in each aligned block of 8 rows (0 to 7, 8 to 15, ...) at most 2 rows name the same one
- member_pick: int32 [256, 4], P('ep'), may hold values from 0 to 7, all different within a row
- picked_probs: float32 [256, 4], P('ep'), may hold values from 0.05 to 1
- gate_weight: bfloat16 [64, 2048, 1024], P('ep', 'tp'), may hold values from -0.125 to 0.125
- up_weight: bfloat16 [64, 2048, 1024], P('ep', 'tp'), may hold values from -0.125 to 0.125
- down_weight: bfloat16 [64, 1024, 2048], P('ep', None, 'tp'), may hold values from -0.375 to 0.375
Outputs:
- mixed: bfloat16 [256, 2048], P('ep', 'tp')
Inputs may be any that keep to these rules, and one draw needn't show every extreme that they name: `group_pick`: each entry is a group number from 0 to 7; within each aligned block of 8 tokens no group is named by more than 2 tokens, a bound that some block reaches. `member_pick`: each token's 4 entries are different member numbers from 0 to 7. `tokens`: each token is its own offset between -2 and 2 plus its own scale between 0.25 and 2 times entries of at most 4 in size.
All inputs are finite; a program needn't handle non-finite values.
Results may differ from a plain program's by a relative error of at most 0.01.
Values may be sent and summed in bfloat16 or wider, within the bound.
No kernel may reach another device: no remote copies, remote signals or barrier semaphores. Data moves between devices by JAX's collectives and lax.ppermute only.
A program may use at most 64 MiB of HBM per device.

v0:
```python
import functools

import jax
import jax.numpy as jnp
from jax import lax
from jax.sharding import Mesh
from jax.sharding import PartitionSpec as P

EPG = 8
TP = ("tp_0", "tp_1")


norm_epsilon = 1e-05


def together(arrays, axis):
    ends = [0]
    for a in arrays:
        ends.append(ends[-1] + a.size)
    subtotal = lax.psum(jnp.concatenate([a.ravel() for a in arrays]), axis)
    return tuple(subtotal[b:e].reshape(a.shape) for a, b, e in zip(arrays, ends, ends[1:]))


def one_axis_at_a_time(x, axes):
    return functools.reduce(lax.psum, axes, x)


def normalize(tokens, norm_gain, norm_bias):
    values = tokens.astype(jnp.float32)
    features = values.shape[1] * lax.axis_size(TP)
    first_sums, square_sums = together(
        (jnp.sum(values, axis=1, keepdims=True), jnp.sum(values * values, axis=1, keepdims=True)),
        TP,
    )
    center = first_sums / features
    shifted = values - center
    spread = square_sums / features - center * center
    scaled = shifted * lax.rsqrt(spread + norm_epsilon)
    return (scaled * norm_gain.astype(jnp.float32) + norm_bias.astype(jnp.float32)).astype(
        jnp.bfloat16
    )


def membership(labels, number):
    levels = lax.broadcasted_iota(jnp.int32, (1, 1, number), 2)
    return jnp.any(labels[:, :, None] == levels, axis=1).astype(jnp.int32)


def earlier_counts(present):
    return (jnp.cumsum(present, axis=0) - present).astype(jnp.int32)


def placement(present, slots, capacity):
    levels = lax.broadcasted_iota(jnp.int32, (1, 1, capacity), 2)
    hits = present[:, :, None] * (slots[:, :, None] == levels).astype(jnp.int32)
    return hits.reshape(present.shape[0], -1).astype(jnp.bfloat16)


def pack_rows(placed, normed):
    return jnp.einsum("tp,td->pd", placed, normed, preferred_element_type=jnp.float32).astype(
        jnp.bfloat16
    )


def activate(gate_full, up_full):
    return (jax.nn.silu(gate_full) * up_full).astype(jnp.bfloat16)


def project_down(hidden, down_weight):
    return jnp.einsum(
        "jrf,jfd->jrd", hidden, down_weight, preferred_element_type=jnp.float32
    ).astype(jnp.bfloat16)


def by_source(results, peers, capacity):
    local_experts = results.shape[0]
    width = results.shape[2]
    parted = results.reshape(local_experts, peers, capacity, width)
    return jnp.transpose(parted, (1, 0, 2, 3)).reshape(peers, local_experts * capacity, width)


def combine(returned, positions, shares):
    picked = jnp.take(returned, positions, axis=0)
    return jnp.sum(shares[:, :, None] * picked.astype(jnp.float32), axis=1).astype(jnp.bfloat16)


def on_device(
    tokens,
    norm_gain,
    norm_bias,
    group_pick,
    member_pick,
    picked_probs,
    gate_weight,
    up_weight,
    down_weight,
):
    normed = normalize(tokens, norm_gain, norm_bias)
    token_count = tokens.shape[0]
    shard_width = tokens.shape[1]
    local_experts = gate_weight.shape[0]
    peers = lax.axis_size("ep")
    experts = local_experts * peers
    groups = experts // EPG
    capacity = max(token_count // 4, (token_count + groups - 1) // groups)
    chosen = (group_pick * EPG + member_pick).astype(jnp.int32)
    shares = picked_probs / jnp.sum(picked_probs, axis=1, keepdims=True)
    present = membership(chosen, experts)
    slots = earlier_counts(present)
    outgoing = pack_rows(placement(present, slots, capacity), normed)
    outgoing = outgoing.reshape(peers, local_experts * capacity, shard_width)
    incoming = lax.all_to_all(outgoing, "ep", split_axis=0, concat_axis=0, tiled=True)
    rows = incoming.reshape(peers, local_experts, capacity, shard_width)
    rows = jnp.transpose(rows, (1, 0, 2, 3)).reshape(local_experts, peers * capacity, shard_width)
    gate_part = jnp.einsum("jrd,jdf->jrf", rows, gate_weight, preferred_element_type=jnp.float32)
    up_part = jnp.einsum("jrd,jdf->jrf", rows, up_weight, preferred_element_type=jnp.float32)
    gate_full, up_full = (one_axis_at_a_time(gate_part, TP), one_axis_at_a_time(up_part, TP))
    results = project_down(activate(gate_full, up_full), down_weight)
    returned = lax.all_to_all(
        by_source(results, peers, capacity), "ep", split_axis=0, concat_axis=0, tiled=True
    )
    positions = chosen * capacity + jnp.take_along_axis(slots, chosen, axis=1)
    mixed = combine(returned.reshape(experts * capacity, shard_width), positions, shares)
    return mixed


def solution(mesh):
    finer = Mesh(mesh.devices.reshape(mesh.shape["ep"], 8, 2), ("ep", "tp_0", "tp_1"))
    placed = (
        P("ep", TP),
        P(TP),
        P(TP),
        P("ep", None),
        P("ep", None),
        P("ep", None),
        P("ep", TP, None),
        P("ep", TP, None),
        P("ep", None, TP),
    )
    return jax.shard_map(
        on_device, mesh=finer, in_specs=placed, out_specs=P("ep", TP), check_vma=False
    )
```

profile of v0, /device:TPU:1, one launch (start us, length us, event | category | flops | bytes accessed | tf_op | source)
XLA Modules:
  0.0 202.2 jit_solution(17553658940312224399)
XLA Ops:
  6.5 0.7 multiply_bitcast_fusion
  7.3 0.8 convert_reduce_fusion
  8.2 29.8 %psum.35 = f32[16]{0:T(128)S(1)} all-reduce(f32[16]{0:T(128)S(1)} %pad_maximum_fusion), channel_id=1, replica_groups=mesh['ep'=32,'tp_0'=8,'tp_1'=2] {'tp_0','tp_1'}, use_global_device_ids=true, to_apply=%region_5.0 | all-reduce | flops 16 | bytes 128 | tf_op jit(solution)/shard_map/psum | solution.py:20
  38.4 0.1 copy.39
  38.5 0.1 copy.38
  38.6 0.1 eq.39
  38.9 0.6 copy-done.4
  39.5 0.2 convolution_convert_fusion.1
  39.7 16.6 %all_to_all.10 = bf16[32,4,128]{2,1,0:T(4,128)(2,1)S(1)} all-to-all(bf16[32,4,128]{2,1,0:T(4,128)(2,1)S(1)} %bitcast.32), channel_id=1, replica_groups=mesh['ep'=32,'tp_0'=8,'tp_1'=2] {'ep'}, dimensions={0} | all-to-all | bytes 65536 | tf_op jit(solution)/shard_map/all_to_all | solution.py:112
  56.4 1.0 fusion.16
  57.5 1.0 fusion.15
  58.6 71.8 %all-reduce.5.cloned.1.call-done = (f32[2,64,1024]{2,1,0:T(8,128)}, f32[2,64,1024]{2,1,0:T(8,128)}) async-done(((f32[2,64,1024]{2,1,0:T(8,128)}, f32[2,64,1024]{2,1,0:T(8,128)}), (f32[2,64,1024]{2,1,0:T(8,128)}, f32[2,64,1024]{2,1,0:T(8,128)})) %all-reduce.5.cloned.1.call-update) | async-done | bytes 1048592 | tf_op jit(solution)/shard_map/psum | solution.py:25
  130.4 0.7 copy-done.2
  131.1 0.1 copy.33
  131.3 0.1 copy.37
  131.4 0.1 reshape.74
  131.4 0.7 gather_fusion.1
  132.3 42.1 %all-reduce.7.cloned.1.call-done = (f32[2,64,1024]{2,1,0:T(8,128)}, f32[2,64,1024]{2,1,0:T(8,128)}) async-done(((f32[2,64,1024]{2,1,0:T(8,128)}, f32[2,64,1024]{2,1,0:T(8,128)}), (f32[2,64,1024]{2,1,0:T(8,128)}, f32[2,64,1024]{2,1,0:T(8,128)})) %all-reduce.7.cloned.1.call-update) | async-done | bytes 1048592 | tf_op jit(solution)/shard_map/psum | solution.py:25
  174.4 1.5 convolution_convert_fusion
  175.9 0.6 copy.42
  176.5 8.9 %all-to-all-start.1 = ((bf16[32,4,128]{2,1,0:T(4,128)(2,1)}), bf16[32,4,128]{2,1,0:T(4,128)(2,1)S(1)}, u32[]{:S(2)}, u32[]{:S(2)}) async-start(bf16[32,4,128]{2,1,0:T(4,128)(2,1)} %copy.42), calls=%async_computation.1 | async-start | bytes 65536 | tf_op jit(solution)/shard_map/all_to_all | solution.py:119
  185.4 8.6 %all-to-all-done.1 = bf16[32,4,128]{2,1,0:T(4,128)(2,1)S(1)} async-done(((bf16[32,4,128]{2,1,0:T(4,128)(2,1)}), bf16[32,4,128]{2,1,0:T(4,128)(2,1)S(1)}, u32[]{:S(2)}, u32[]{:S(2)}) %all-to-all-start.1) | async-done | bytes 32800 | tf_op jit(solution)/shard_map/all_to_all | solution.py:119
  194.0 0.6 gather_fusion
  194.6 0.7 multiply_reduce_fusion
  (40 shorter events, 1.0 us)
Async XLA Ops:
  6.5 49.9 %copy-start = (bf16[2,128,1024]{2,1,0:T(8,128)(2,1)S(1)}, bf16[2,128,1024]{2,1,0:T(8,128)(2,1)}, u32[]{:S(2)}) copy-start(bf16[2,128,1024]{2,1,0:T(8,128)(2,1)} %param.16) | copy-start | bytes 1572868
  6.5 123.8 %all-reduce.5.cloned.1.call-start = ((), (), s32[]{:S(2)}) async-start(), calls=%async_computation.2 | async-start | bytes 2097152 | tf_op jit(solution)/shard_map/psum | solution.py:25
  8.2 29.9 %copy-start.3 = (s32[8,4]{0,1:T(4,128)S(1)}, s32[8,4]{0,1:T(4,128)}, u32[]{:S(2)}) copy-start(s32[8,4]{0,1:T(4,128)} %param.13) | copy-start | bytes 388
  38.8 0.7 copy-start.4
  38.8 0.7 copy-start.6
  38.8 0.7 copy-start.7
  56.4 1.1 copy-start.1
  58.5 115.9 %all-reduce.7.cloned.1.call-start = ((), (), s32[]{:S(2)}) async-start(), calls=%async_computation.3 | async-start | bytes 2097152 | tf_op jit(solution)/shard_map/psum | solution.py:25
  130.4 0.7 copy-start.2
  131.4 42.9 %copy-start.5 = (bf16[2,1024,128]{2,1,0:T(8,128)(2,1)S(1)}, bf16[2,1024,128]{2,1,0:T(8,128)(2,1)}, u32[]{:S(2)}) copy-start(bf16[2,1024,128]{2,1,0:T(8,128)(2,1)} %param.17) | copy-start | bytes 1572868
  176.5 17.5 %all-to-all-start.1 = ((bf16[32,4,128]{2,1,0:T(4,128)(2,1)}), bf16[32,4,128]{2,1,0:T(4,128)(2,1)S(1)}, u32[]{:S(2)}, u32[]{:S(2)}) async-start(bf16[32,4,128]{2,1,0:T(4,128)(2,1)} %copy.42), calls=%async_computation.1 | async-start | bytes 65536 | tf_op jit(solution)/shard_map/all_to_all | solution.py:119
Sparse Core Ops, SparseCore 0:
  58.6 71.7 all-reduce.4
  133.3 41.0 all-reduce.6
where the time goes:
time: 203 us; the launch traced here: 202 us
  waiting for transfers between devices  123 us (61%)
  blocking collectives  46.5 us (23%)
  between operations  13.5 us (7%)
  starting transfers between devices  8.95 us (4%)
  local copies, waits for them, and re-layouts  4.28 us (2%)
  matrix products  3.75 us (2%)
  other arithmetic  2.62 us (1%)
    psum x2, waiting for transfers between devices, one_axis_at_a_time(): return functools.reduce(lax.psum, axes, x)  114 us
    psum x1, blocking collectives, together(): subtotal = lax.psum(jnp.concatenate([a.ravel() for a in arrays]), axis)  29.8 us
    all_to_all x1, blocking collectives, on_device(): lax.all_to_all(outgoing, 'ep', split_axis=0, concat_axis=0, tiled=True)  16.6 us
    all_to_all x1, starting transfers between devices, on_device(): lax.all_to_all(by_source(results, peers, capacity), 'ep', split_axis=0, c...  8.9 us
    all_to_all x1, waiting for transfers between devices, on_device(): lax.all_to_all(by_source(results, peers, capacity), 'ep', split_axis=0, c...  8.62 us
  transfers between devices with their start and end apart: 3, of which 3 were waited for; matrix products, arithmetic and copies ran while one was open for 1% of the time, Pallas kernels for 0%

commit v1 on v0

v1 whole, which is shorter than its diff:
```python
import functools

import jax
import jax.numpy as jnp
from jax import lax
from jax.experimental import pallas as pl
from jax.experimental.pallas import tpu as pltpu
from jax.sharding import Mesh
from jax.sharding import PartitionSpec as P

f32 = jnp.float32
bf16 = jnp.bfloat16

EPG = 8
SLOTS = 2
LANES = 128
NORM_EPSILON = 1e-05

VMEM = pl.BlockSpec(memory_space=pltpu.VMEM)
SMEM = pl.BlockSpec(memory_space=pltpu.SMEM)


def call(body, out_shape, in_specs, flops=0, moved=0):
    specs = jax.tree.map(lambda _: VMEM, out_shape)
    return pl.pallas_call(
        body,
        out_shape=out_shape,
        in_specs=in_specs,
        out_specs=specs,
        cost_estimate=pl.CostEstimate(flops=flops, bytes_accessed=moved, transcendentals=0),
    )


def shape(dims, dtype=bf16):
    return jax.ShapeDtypeStruct(dims, dtype)


def three(value):
    high = value.astype(bf16).astype(f32)
    middle = (value - high).astype(bf16).astype(f32)
    low = (value - high - middle).astype(bf16).astype(f32)
    return high, middle, low


def iota(dims, axis):
    return lax.broadcasted_iota(jnp.int32, dims, axis)


def by_row(rows, width):
    at = iota((8, width), 0)
    out = jnp.zeros((8, width), f32)
    for i, row in enumerate(rows):
        out = jnp.where(at == i, jnp.broadcast_to(row, (8, width)), out)
    return out


def dot(a, b):
    return jnp.dot(a, b, preferred_element_type=f32)


def slots_of(groups):
    count = groups.shape[1]
    at = iota((1, count), 1)
    slots = jnp.zeros((1, count), jnp.int32)
    for j in range(count - 1):
        same = jnp.broadcast_to(groups[:, j : j + 1], (1, count)) == groups
        slots = slots + jnp.where(same & (at > j), 1, 0)
    return slots


def share_body(tokens, gain, bias, out):
    out[0:8, :] = tokens[...]
    rows = three(gain[...]) + three(bias[...])
    out[8:16, :] = by_row(rows, LANES).astype(bf16)


def pack_body(core, both, groups, out, affine):
    first, second = both[0].astype(f32), both[1].astype(f32)
    lower = core[0] == 0
    own, other = jnp.where(lower, first, second), jnp.where(lower, second, first)
    affine[:, 0:LANES] = own[8:16].astype(bf16)
    affine[:, LANES:] = other[8:16].astype(bf16)
    values = jnp.concatenate([own[0:8], other[0:8]], axis=0).astype(bf16)
    place = out.shape[0]
    per = place // 8
    chosen = groups[...]
    slots = slots_of(chosen)
    pair = jnp.concatenate([chosen, chosen], axis=1)
    slot_pair = jnp.concatenate([slots, slots], axis=1)
    row = iota((place, 16), 0)
    half = jnp.where(iota((place, 16), 1) >= 8, 1, 0)
    hit = (
        (row // per == pair)
        & (row % SLOTS == slot_pair)
        & ((row // SLOTS) % 2 == half)
    )
    out[...] = dot(jnp.where(hit, 1.0, 0.0).astype(bf16), values).astype(bf16)


def spread_body(arrived, affine, own, received, out):
    places = arrived.shape[0]
    rows = places // 2
    at, source = iota((rows, places), 0), iota((rows, places), 1)
    values = arrived[...]
    halves = []
    for half in range(2):
        takes = source == (at // SLOTS) * (2 * SLOTS) + half * SLOTS + at % SLOTS
        halves.append(dot(jnp.where(takes, 1.0, 0.0).astype(bf16), values))
    features = 2 * LANES
    mean = (
        jnp.sum(halves[0], axis=1, keepdims=True) + jnp.sum(halves[1], axis=1, keepdims=True)
    ) / features
    centred = [h - mean for h in halves]
    square = jnp.sum(centred[0] * centred[0] + centred[1] * centred[1], axis=1, keepdims=True)

    lane = iota((rows, LANES), 1)
    stats = jnp.where(lane == 0, mean, jnp.where(lane == 1, square, 0.0))
    stats = jnp.concatenate([stats, jnp.zeros((LANES - rows, LANES), f32)], axis=0).T
    means, squares = three(stats[0:1]), three(stats[1:2])

    left = []
    for half in range(2):
        lanes = slice(half * LANES, (half + 1) * LANES)
        affine_rows = affine[:, lanes]
        wide = affine_rows.astype(f32)
        gain = wide[0:1] + wide[1:2] + wide[2:3]
        left.append(jnp.concatenate([(centred[half] * gain).astype(bf16), affine_rows], axis=0))

    for mat, stat in ((0, means), (1, squares)):
        total = dot(left[0], own[mat]) + dot(left[1], received[mat])
        tail = total[rows : rows + 8]
        gain_sum = tail[0:1] + tail[1:2] + tail[2:3]
        bias_sum = tail[3:4] + tail[4:5] + tail[5:6]
        parts = three(gain_sum)[0:2] + three(bias_sum)[0:2]
        for y in range(out.shape[0]):
            lanes = slice(y * LANES, (y + 1) * LANES)
            put = slice(mat * LANES, (mat + 1) * LANES)
            out[y, 0:rows, put] = total[0:rows, lanes].astype(bf16)
            out[y, rows : rows + 8, put] = by_row([p[:, lanes] for p in parts] + list(stat), LANES).astype(bf16)


def activate_body(features, parts, out):
    peers = parts.shape[0]
    rows = parts.shape[1] - 8
    tails = [parts[s, rows : rows + 8, :].astype(f32) for s in range(peers)]
    means = by_row([t[4:5, 0:LANES] + t[5:6, 0:LANES] + t[6:7, 0:LANES] for t in tails], LANES)
    squares = by_row([t[4:5, LANES:] + t[5:6, LANES:] + t[6:7, LANES:] for t in tails], LANES)
    center = jnp.sum(means, axis=0, keepdims=True) / peers
    shift = means - center
    spread = jnp.sum(squares + (features // peers) * shift * shift, axis=0, keepdims=True) / features
    scale = jnp.broadcast_to(lax.rsqrt(spread + NORM_EPSILON), (8, LANES))
    turned = jnp.concatenate([shift, scale, jnp.zeros((LANES - 16, LANES), f32)], axis=0).T

    sums = parts[0, 0:rows, :].astype(f32)
    for s in range(1, peers):
        sums = sums + parts[s, 0:rows, :].astype(f32)
    bias = tails[0][2:3] + tails[0][3:4]
    for s in range(peers):
        sums = sums + turned[0:rows, s : s + 1] * (tails[s][0:1] + tails[s][1:2])
        if s:
            bias = bias + tails[s][2:3] + tails[s][3:4]
    full = turned[0:rows, 8:9] * sums + bias
    gate, up = full[:, 0:LANES], full[:, LANES:]
    hidden = (gate / (1.0 + jnp.exp(-gate)) * up).astype(bf16)
    for s in range(peers):
        out[s] = hidden


def project_body(hidden, down, out):
    experts, tiles, rows, width = hidden.shape
    places = out.shape[0]
    row, source = iota((places, rows), 0), iota((places, rows), 1)
    total = jnp.zeros((places, LANES), f32)
    for e in range(experts):
        wide = jnp.concatenate([hidden[e, y] for y in range(tiles)], axis=1)
        result = dot(wide, down[e]).astype(bf16)
        puts = row == (source // SLOTS) * (2 * SLOTS) + e * SLOTS + source % SLOTS
        total = total + dot(jnp.where(puts, 1.0, 0.0).astype(bf16), result)
    out[...] = total.astype(bf16)


def combine_body(returned, groups, members, probs, out):
    places = returned.shape[0]
    count = groups.shape[1]
    chosen = groups[...]
    slots = slots_of(chosen)
    likely = probs[...]
    shares = likely / jnp.sum(likely, axis=0, keepdims=True)
    row = iota((places, count), 0)
    weights = jnp.zeros((places, count), f32)
    for k in range(members.shape[0]):
        member = members[k : k + 1, :]
        place = (chosen * (EPG // 2) + member // 2) * (2 * SLOTS) + (member % 2) * SLOTS + slots
        weights = weights + jnp.where(row == place, shares[k : k + 1, :], 0.0)
    values = returned[...]
    total = jnp.zeros((count, LANES), f32)
    for part in three(weights):
        total = total + lax.dot_general(
            part.astype(bf16), values, (((0,), (0,)), ((), ())), preferred_element_type=f32
        )
    out[...] = total.astype(bf16)


def on_device(
    tokens,
    norm_gain,
    norm_bias,
    group_pick,
    member_pick,
    picked_probs,
    gate_weight,
    up_weight,
    down_weight,
):
    ep = ("z", "x")
    peers = lax.axis_size(ep)
    tiles = lax.axis_size("y")
    count, width = tokens.shape
    inner = gate_weight.shape[2]
    rows = peers * SLOTS
    places = 2 * rows
    features = width * tiles * 2
    core = lax.axis_index("c")
    groups, members, probs = group_pick.T, member_pick.T, picked_probs.T

    pick = lambda w, i: lax.dynamic_index_in_dim(w, i, 0, keepdims=False)
    sent = jnp.stack([pick(gate_weight, 1 - core), pick(up_weight, 1 - core)])
    received = lax.ppermute(sent, "c", [(0, 1), (1, 0)])
    own = jnp.stack([pick(gate_weight, core), pick(up_weight, core)])

    mine = call(share_body, shape((16, LANES)), [VMEM] * 3)(
        tokens, norm_gain.reshape(1, width), norm_bias.reshape(1, width)
    )
    both = lax.all_gather(mine, "c", axis=0, tiled=False)
    outgoing, affine = call(
        pack_body, (shape((places, LANES)), shape((8, 2 * LANES))), [SMEM, VMEM, VMEM]
    )(core.reshape(1), both, groups)
    arrived = lax.all_to_all(
        outgoing.reshape(peers, 2 * SLOTS, LANES), ep, split_axis=0, concat_axis=0, tiled=True
    ).reshape(places, LANES)

    parts = call(
        spread_body,
        shape((tiles, rows + 8, 2 * LANES)),
        [VMEM] * 4,
        flops=2 * (rows + 8) * 2 * width * 2 * inner,
        moved=own.size * 4,
    )(arrived, affine, own, received)
    parts = lax.all_to_all(parts, "y", split_axis=0, concat_axis=0, tiled=True)
    hidden = call(functools.partial(activate_body, features), shape((tiles, rows, LANES)), [VMEM])(parts)
    hidden = lax.all_to_all(hidden, "y", split_axis=0, concat_axis=0, tiled=True)
    hidden = lax.all_gather(hidden, "c", axis=0, tiled=False)
    results = call(
        project_body,
        shape((places, LANES)),
        [VMEM] * 2,
        flops=2 * rows * 2 * inner * width,
        moved=down_weight.size * 2,
    )(hidden, down_weight)
    returned = lax.all_to_all(
        results.reshape(peers, 2 * SLOTS, LANES), ep, split_axis=0, concat_axis=0, tiled=True
    ).reshape(places, LANES)
    return call(combine_body, shape((count, LANES)), [VMEM] * 4)(returned, groups, members, probs)


def solution(mesh):
    finer = Mesh(mesh.devices.reshape(8, 4, 8, 2), ("z", "x", "y", "c"))
    ep, tp = ("z", "x"), ("y", "c")
    placed = (
        P(ep, tp),
        P(tp),
        P(tp),
        P(ep, None),
        P(ep, None),
        P(ep, None),
        P(ep, tp, None),
        P(ep, tp, None),
        P(ep, None, tp),
    )
    return jax.shard_map(
        on_device, mesh=finer, in_specs=placed, out_specs=P(ep, tp), check_vma=False
    )
```

time: 203 us -> 88.6 us (0.44)
  waiting for transfers between devices: 123 us -> 7.8 us
  between operations: 13.5 us -> 0.04 us
  Pallas kernels: 0 us -> 11.1 us
  starting transfers between devices: 8.95 us -> 16.3 us
  matrix products: 3.75 us -> 0 us
  blocking collectives: 46.5 us -> 49.7 us
  local copies, waits for them, and re-layouts: 4.28 us -> 2.08 us
    psum x2 -> x0, waiting for transfers between devices: 114 us -> none  [one_axis_at_a_time(): return functools.reduce(lax.psum, axes, x)]
    psum x1 -> x0, blocking collectives: 29.8 us -> none  [together(): subtotal = lax.psum(jnp.concatenate([a.ravel() for a in arrays]), axis)]
    all_to_all x1 -> x3, blocking collectives: 16.6 us -> 42.2 us  [the longest x1 15.3 us: on_device(): parts = lax.all_to_all(parts, 'y', split_axis=0, concat_axis=0, tiled=True)]
    pallas_call x0 -> x6, Pallas kernels: none -> 11.1 us  [the longest x1 2.49 us: on_device(): call(spread_body, shape((tiles, rows + 8, 2 * LANES)), [VMEM] * 4, flops=...]
    ppermute x0 -> x1, starting transfers between devices: none -> 8.72 us  [on_device(): received = lax.ppermute(sent, 'c', [(0, 1), (1, 0)])]
    all_gather x0 -> x2, blocking collectives: none -> 7.46 us  [the longest x1 4.4 us: on_device(): hidden = lax.all_gather(hidden, 'c', axis=0, tiled=False)]
    dot_general x4 -> x0, matrix products: 3.75 us -> none  [the longest x1 1.48 us: project_down(): jnp.einsum('jrf,jfd->jrd', hidden, down_weight, preferred_element_type=jn...]
  transfers between devices with their start and end apart: 3 -> 2, of which waited for: 3 -> 1; matrix products, arithmetic and copies ran while one was open for 1% -> 1% of each run, Pallas kernels for 0% -> 3%
where the time goes in v1:
time: 88.6 us; the launch traced here: 87.9 us
  blocking collectives  49.7 us (56%)
  starting transfers between devices  16.3 us (18%)
  Pallas kernels  11.1 us (13%)
  waiting for transfers between devices  7.8 us (9%)
  local copies, waits for them, and re-layouts  2.08 us (2%)
  other arithmetic  0.89 us (1%)
    all_to_all x1, blocking collectives, on_device(): parts = lax.all_to_all(parts, 'y', split_axis=0, concat_axis=0, tiled=True)  15.3 us
    all_to_all x1, blocking collectives, on_device(): lax.all_to_all(hidden, 'y', split_axis=0, concat_axis=0, tiled=True)  13.8 us
    all_to_all x1, blocking collectives, on_device(): lax.all_to_all(results.reshape(peers, 2 * SLOTS, LANES), ep, split_axis=0...  13.1 us
    ppermute x1, starting transfers between devices, on_device(): received = lax.ppermute(sent, 'c', [(0, 1), (1, 0)])  8.72 us
    all_to_all x1, waiting for transfers between devices, on_device(): lax.all_to_all(outgoing.reshape(peers, 2 * SLOTS, LANES), ep, split_axis=...  7.79 us
    all_to_all x1, starting transfers between devices, on_device(): lax.all_to_all(outgoing.reshape(peers, 2 * SLOTS, LANES), ep, split_axis=...  7.58 us
    all_gather x1, blocking collectives, on_device(): hidden = lax.all_gather(hidden, 'c', axis=0, tiled=False)  4.4 us
    all_gather x1, blocking collectives, on_device(): both = lax.all_gather(mine, 'c', axis=0, tiled=False)  3.06 us
  transfers between devices with their start and end apart: 2, of which 1 were waited for; matrix products, arithmetic and copies ran while one was open for 1% of the time, Pallas kernels for 3%

profile of v1, /device:TPU:1, one launch (start us, length us, event | category | flops | bytes accessed | tf_op | source)
XLA Modules:
  0.0 87.9 jit_solution(3694657173284861653)
XLA Ops:
  0.0 1.3 %constant_dynamic-slice_fusion = (bf16[1,128,1024]{2,1,0:T(8,128)(2,1)S(1)}, bf16[1,128,1024]{2,1,0:T(8,128)(2,1)S(1)}, bf16[1,128,1024]{2,1,0:T(8,128)(2,1)S(1)}, bf16[1,128,1024]{2,1,0:T(8,128)(2,1)S(1)}) fusion(bf16[2,128,1024]{2,1,0:T(8,128)(2,1)} %param.16, s32[]{:T(128)S(6)} %select_n.10, s32[]{:T(128)S(6)} %select_n.9, bf16[2,128,1024]{2,1,0:T(8,128)(2,1)} %param.15), kind=kLoop, calls=%fused_computation.2 | loop fusion | bytes 2097160 | tf_op jit(solution)/shard_map/jit(dynamic_index_in_dim)/dynamic_slice | solution.py:226
  1.3 0.1 pad_maximum_fusion.1
  1.3 8.7 %collective-permute-start = (bf16[2,128,1024]{2,1,0:T(8,128)(2,1)S(1)}, bf16[2,128,1024]{2,1,0:T(8,128)(2,1)S(1)}, u32[]{:S(2)}, u32[]{:S(2)}) collective-permute-start(bf16[2,128,1024]{2,1,0:T(8,128)(2,1)S(1)} %pad_maximum_fusion.1), channel_id=1, source_target_pairs={{0,1},{1,0},{2,3},{3,2},{4,5},{5,4},{6,7},{7,6},{8,9},{9,8},{10,11... | collective-permute-start | bytes 1572872 | tf_op jit(solution)/shard_map/ppermute | solution.py:228
  10.1 1.3 %shard_map.91 = bf16[16,128]{1,0:T(8,128)(2,1)} custom-call(bf16[8,128]{1,0:T(8,128)(2,1)} %tokens.1, f32[1,128]{1,0:T(1,128)} %bitcast.22, f32[1,128]{1,0:T(1,128)} %bitcast.23), custom_call_target="tpu_custom_call" | custom-call | tf_op jit(solution)/shard_map/pallas_call | solution.py:231
  11.4 3.1 %all-gather = bf16[32,128]{1,0:T(8,128)(2,1)} all-gather(bf16[16,128]{1,0:T(8,128)(2,1)} %shard_map.91), channel_id=2, replica_groups=mesh['z'=8,'x'=4,'y'=8,'c'=2] {'c'}, dimensions={0}, use_global_device_ids=true | all-gather | bytes 12288 | tf_op jit(solution)/shard_map/all_gather | solution.py:234
  14.4 1.6 %shard_map.92 = (bf16[128,128]{1,0:T(8,128)(2,1)}, bf16[8,256]{1,0:T(8,128)(2,1)}) custom-call(s32[1]{0:T(128)} %bitcast.core, bf16[2,16,128]{2,1,0:T(8,128)(2,1)} %bitcast.16, s32[1,8]{1,0:T(1,128)} %bitcast.18), custom_call_target="tpu_custom_call" | custom-call | tf_op jit(solution)/shard_map/pallas_call | solution.py:235
  16.0 7.6 %all-to-all-start = ((bf16[32,4,128]{2,1,0:T(4,128)(2,1)}), bf16[32,4,128]{2,1,0:T(4,128)(2,1)S(1)}, u32[]{:S(2)}, u32[]{:S(2)}) async-start(bf16[32,4,128]{2,1,0:T(4,128)(2,1)} %bitcast.17), calls=%async_computation | async-start | bytes 65536 | tf_op jit(solution)/shard_map/all_to_all | solution.py:238
  23.6 0.8 pad_maximum_fusion.own
  24.5 7.8 %all-to-all-done = bf16[32,4,128]{2,1,0:T(4,128)(2,1)S(1)} async-done(((bf16[32,4,128]{2,1,0:T(4,128)(2,1)}), bf16[32,4,128]{2,1,0:T(4,128)(2,1)S(1)}, u32[]{:S(2)}, u32[]{:S(2)}) %all-to-all-start) | async-done | bytes 32800 | tf_op jit(solution)/shard_map/all_to_all | solution.py:238
  32.3 0.0 copy-start.1
  32.3 0.0 collective-permute-done.received
  32.3 0.0 copy-start
  32.3 0.6 copy-done.1
  32.9 0.2 copy-done
  33.1 2.5 %shard_map.93 = bf16[8,72,256]{2,1,0:T(8,128)(2,1)} custom-call(bf16[128,128]{1,0:T(8,128)(2,1)} %bitcast.13, bf16[8,256]{1,0:T(8,128)(2,1)} %get-tuple-element.8.affine, bf16[2,128,1024]{2,1,0:T(8,128)(2,1)} %pad_maximum_fusion.own, bf16[2,128,1024]{2,1,0:T(8,128)(2,1)} %copy-done), custom_call_target="tpu_custom_call" | custom-call | flops 75497472 | bytes 1048576 | tf_op jit(solution)/shard_map/pallas_call | solution.py:242
  35.6 15.3 %all_to_all.20.parts = bf16[8,72,256]{2,1,0:T(8,128)(2,1)} all-to-all(bf16[8,72,256]{2,1,0:T(8,128)(2,1)} %shard_map.93), channel_id=1, replica_groups=mesh['z'=8,'x'=4,'y'=8,'c'=2] {'y'}, dimensions={0} | all-to-all | bytes 589824 | tf_op jit(solution)/shard_map/all_to_all | solution.py:249
  50.8 1.9 %shard_map.94 = bf16[8,64,128]{2,1,0:T(8,128)(2,1)} custom-call(bf16[8,72,256]{2,1,0:T(8,128)(2,1)} %all_to_all.20.parts), custom_call_target="tpu_custom_call" | custom-call | tf_op jit(solution)/shard_map/pallas_call | solution.py:250
  52.8 13.8 %all_to_all.21 = bf16[8,64,128]{2,1,0:T(8,128)(2,1)S(1)} all-to-all(bf16[8,64,128]{2,1,0:T(8,128)(2,1)} %shard_map.94), channel_id=1, replica_groups=mesh['z'=8,'x'=4,'y'=8,'c'=2] {'y'}, dimensions={0} | all-to-all | bytes 262144 | tf_op jit(solution)/shard_map/all_to_all | solution.py:251
  66.6 4.4 %all-gather.1 = bf16[16,64,128]{2,1,0:T(8,128)(2,1)} all-gather(bf16[8,64,128]{2,1,0:T(8,128)(2,1)S(1)} %all_to_all.21), channel_id=3, replica_groups=mesh['z'=8,'x'=4,'y'=8,'c'=2] {'c'}, dimensions={0}, use_global_device_ids=true | all-gather | bytes 393216 | tf_op jit(solution)/shard_map/all_gather | solution.py:252
  71.0 2.1 %shard_map.95 = bf16[128,128]{1,0:T(8,128)(2,1)} custom-call(bf16[2,8,64,128]{3,2,1,0:T(8,128)(2,1)} %bitcast.12, bf16[2,1024,128]{2,1,0:T(8,128)(2,1)} %down.1), custom_call_target="tpu_custom_call" | custom-call | flops 33554432 | bytes 524288 | tf_op jit(solution)/shard_map/pallas_call | solution.py:253
  73.1 13.1 %all_to_all.22 = bf16[32,4,128]{2,1,0:T(4,128)(2,1)} all-to-all(bf16[32,4,128]{2,1,0:T(4,128)(2,1)} %bitcast.14), channel_id=1, replica_groups=mesh['z'=8,'x'=4,'y'=8,'c'=2] {'z','x'}, dimensions={0} | all-to-all | bytes 65536 | tf_op jit(solution)/shard_map/all_to_all | solution.py:260
  86.2 1.6 %shard_map.96 = bf16[8,128]{1,0:T(8,128)(2,1)} custom-call(bf16[128,128]{1,0:T(8,128)(2,1)} %bitcast.15, s32[1,8]{1,0:T(1,128)} %bitcast.19, s32[4,8]{1,0:T(4,128)} %bitcast.20, f32[4,8]{1,0:T(4,128)} %bitcast.21), custom_call_target="tpu_custom_call" | custom-call | tf_op jit(solution)/shard_map/pallas_call | solution.py:263
Async XLA Ops:
  1.3 30.9 %collective-permute-start = (bf16[2,128,1024]{2,1,0:T(8,128)(2,1)S(1)}, bf16[2,128,1024]{2,1,0:T(8,128)(2,1)S(1)}, u32[]{:S(2)}, u32[]{:S(2)}) collective-permute-start(bf16[2,128,1024]{2,1,0:T(8,128)(2,1)S(1)} %pad_maximum_fusion.1), channel_id=1, source_target_pairs={{0,1},{1,0},{2,3},{3,2},{4,5},{5,4},{6,7},{7,6},{8,9},{9,8},{10,11... | collective-permute-start | bytes 1572872 | tf_op jit(solution)/shard_map/ppermute | solution.py:228
  16.0 16.2 %all-to-all-start = ((bf16[32,4,128]{2,1,0:T(4,128)(2,1)}), bf16[32,4,128]{2,1,0:T(4,128)(2,1)S(1)}, u32[]{:S(2)}, u32[]{:S(2)}) async-start(bf16[32,4,128]{2,1,0:T(4,128)(2,1)} %bitcast.17), calls=%async_computation | async-start | bytes 65536 | tf_op jit(solution)/shard_map/all_to_all | solution.py:238
  32.3 0.6 copy-start.1
  32.3 0.8 copy-start

commit v2 on v1

--- a/solution.py
+++ b/solution.py
@@ -18,21 +18,32 @@
 
 VMEM = pl.BlockSpec(memory_space=pltpu.VMEM)
 SMEM = pl.BlockSpec(memory_space=pltpu.SMEM)
-
-
-def call(body, out_shape, in_specs, flops=0, moved=0):
+ANY = pl.BlockSpec(memory_space=pl.ANY)
+
+
+def call(body, out_shape, in_specs, flops=0, moved=0, scratch=()):
     specs = jax.tree.map(lambda _: VMEM, out_shape)
-    return pl.pallas_call(
+    kernel = pl.pallas_call(
         body,
         out_shape=out_shape,
         in_specs=in_specs,
         out_specs=specs,
+        scratch_shapes=scratch,
         cost_estimate=pl.CostEstimate(flops=flops, bytes_accessed=moved, transcendentals=0),
     )
 
+    def run(*args):
+        near = [
+            pltpu.with_memory_space_constraint(a, pltpu.VMEM) if spec is VMEM else a
+            for a, spec in zip(args, in_specs)
+        ]
+        return kernel(*near)
+
+    return run
+
 
 def shape(dims, dtype=bf16):
-    return jax.ShapeDtypeStruct(dims, dtype)
+    return pltpu.VMEM(dims, dtype)
 
 
 def three(value):
@@ -68,22 +79,30 @@
     return slots
 
 
-def share_body(tokens, gain, bias, out):
-    out[0:8, :] = tokens[...]
-    rows = three(gain[...]) + three(bias[...])
+def share_body(core, tokens, gain, bias, groups, members, probs, gate, up, out, sent, hits, weights, *scratch):
+    near_gain, near_bias, near_groups, near_members, near_probs, arrived = scratch
+    peer = 1 - core[0]
+    pairs = (
+        (gain, near_gain),
+        (bias, near_bias),
+        (groups, near_groups),
+        (members, near_members),
+        (probs, near_probs),
+        (tokens, out.at[0:8]),
+        (gate.at[peer], sent.at[0]),
+        (up.at[peer], sent.at[1]),
+    )
+    copies = [pltpu.make_async_copy(a, b, arrived.at[i]) for i, (a, b) in enumerate(pairs)]
+    for copy in copies:
+        copy.start()
+    for copy in copies[0:5]:
+        copy.wait()
+    rows = three(near_gain[...]) + three(near_bias[...])
     out[8:16, :] = by_row(rows, LANES).astype(bf16)
 
-
-def pack_body(core, both, groups, out, affine):
-    first, second = both[0].astype(f32), both[1].astype(f32)
-    lower = core[0] == 0
-    own, other = jnp.where(lower, first, second), jnp.where(lower, second, first)
-    affine[:, 0:LANES] = own[8:16].astype(bf16)
-    affine[:, LANES:] = other[8:16].astype(bf16)
-    values = jnp.concatenate([own[0:8], other[0:8]], axis=0).astype(bf16)
-    place = out.shape[0]
+    place = hits.shape[0]
     per = place // 8
-    chosen = groups[...]
+    chosen = near_groups[...]
     slots = slots_of(chosen)
     pair = jnp.concatenate([chosen, chosen], axis=1)
     slot_pair = jnp.concatenate([slots, slots], axis=1)
@@ -94,10 +113,32 @@
         & (row % SLOTS == slot_pair)
         & ((row // SLOTS) % 2 == half)
     )
-    out[...] = dot(jnp.where(hit, 1.0, 0.0).astype(bf16), values).astype(bf16)
-
-
-def spread_body(arrived, affine, own, received, out):
+    hits[...] = jnp.where(hit, 1.0, 0.0).astype(bf16)
+
+    likely = near_probs[...]
+    shares = likely / jnp.sum(likely, axis=0, keepdims=True)
+    row = iota((place, 8), 0)
+    total = jnp.zeros((place, 8), f32)
+    for k in range(members.shape[0]):
+        member = near_members[k : k + 1, :]
+        at = (chosen * (EPG // 2) + member // 2) * (2 * SLOTS) + (member % 2) * SLOTS + slots
+        total = total + jnp.where(row == at, shares[k : k + 1, :], 0.0)
+    weights[...] = total
+    for copy in copies[5:]:
+        copy.wait()
+
+
+def pack_body(core, both, hits, out, affine):
+    first, second = both[0].astype(f32), both[1].astype(f32)
+    lower = core[0] == 0
+    own, other = jnp.where(lower, first, second), jnp.where(lower, second, first)
+    affine[:, 0:LANES] = own[8:16].astype(bf16)
+    affine[:, LANES:] = other[8:16].astype(bf16)
+    values = jnp.concatenate([own[0:8], other[0:8]], axis=0).astype(bf16)
+    out[...] = dot(hits[...], values).astype(bf16)
+
+
+def spread_body(core, arrived, affine, gate, up, received, out):
     places = arrived.shape[0]
     rows = places // 2
     at, source = iota((rows, places), 0), iota((rows, places), 1)
@@ -127,7 +168,8 @@
         left.append(jnp.concatenate([(centred[half] * gain).astype(bf16), affine_rows], axis=0))
 
     for mat, stat in ((0, means), (1, squares)):
-        total = dot(left[0], own[mat]) + dot(left[1], received[mat])
+        own = (gate, up)[mat][core[0]]
+        total = dot(left[0], own) + dot(left[1], received[mat])
         tail = total[rows : rows + 8]
         gain_sum = tail[0:1] + tail[1:2] + tail[2:3]
         bias_sum = tail[3:4] + tail[4:5] + tail[5:6]
@@ -179,22 +221,10 @@
     out[...] = total.astype(bf16)
 
 
-def combine_body(returned, groups, members, probs, out):
-    places = returned.shape[0]
-    count = groups.shape[1]
-    chosen = groups[...]
-    slots = slots_of(chosen)
-    likely = probs[...]
-    shares = likely / jnp.sum(likely, axis=0, keepdims=True)
-    row = iota((places, count), 0)
-    weights = jnp.zeros((places, count), f32)
-    for k in range(members.shape[0]):
-        member = members[k : k + 1, :]
-        place = (chosen * (EPG // 2) + member // 2) * (2 * SLOTS) + (member % 2) * SLOTS + slots
-        weights = weights + jnp.where(row == place, shares[k : k + 1, :], 0.0)
+def combine_body(returned, weights, out):
     values = returned[...]
-    total = jnp.zeros((count, LANES), f32)
-    for part in three(weights):
+    total = jnp.zeros(out.shape, f32)
+    for part in three(weights[...]):
         total = total + lax.dot_general(
             part.astype(bf16), values, (((0,), (0,)), ((), ())), preferred_element_type=f32
         )
@@ -223,18 +253,40 @@
     core = lax.axis_index("c")
     groups, members, probs = group_pick.T, member_pick.T, picked_probs.T
 
-    pick = lambda w, i: lax.dynamic_index_in_dim(w, i, 0, keepdims=False)
-    sent = jnp.stack([pick(gate_weight, 1 - core), pick(up_weight, 1 - core)])
+    at = core.reshape(1)
+    mine, sent, hits, weights = call(
+        share_body,
+        (
+            shape((16, LANES)),
+            shape((2, width, inner)),
+            shape((places, 2 * count)),
+            shape((places, count), f32),
+        ),
+        [SMEM] + [ANY] * 8,
+        scratch=[
+            pltpu.VMEM((1, width), f32),
+            pltpu.VMEM((1, width), f32),
+            pltpu.VMEM(groups.shape, groups.dtype),
+            pltpu.VMEM(members.shape, members.dtype),
+            pltpu.VMEM(probs.shape, probs.dtype),
+            pltpu.SemaphoreType.DMA((8,)),
+        ],
+    )(
+        at,
+        tokens,
+        norm_gain.reshape(1, width),
+        norm_bias.reshape(1, width),
+        groups,
+        members,
+        probs,
+        gate_weight,
+        up_weight,
+    )
     received = lax.ppermute(sent, "c", [(0, 1), (1, 0)])
-    own = jnp.stack([pick(gate_weight, core), pick(up_weight, core)])
-
-    mine = call(share_body, shape((16, LANES)), [VMEM] * 3)(
-        tokens, norm_gain.reshape(1, width), norm_bias.reshape(1, width)
-    )
     both = lax.all_gather(mine, "c", axis=0, tiled=False)
     outgoing, affine = call(
-        pack_body, (shape((places, LANES)), shape((8, 2 * LANES))), [SMEM, VMEM, VMEM]
-    )(core.reshape(1), both, groups)
+        pack_body, (shape((places, LANES)), shape((8, 2 * LANES))), [SMEM] + [VMEM] * 2
+    )(at, both, hits)
     arrived = lax.all_to_all(
         outgoing.reshape(peers, 2 * SLOTS, LANES), ep, split_axis=0, concat_axis=0, tiled=True
     ).reshape(places, LANES)
@@ -242,10 +294,10 @@
     parts = call(
         spread_body,
         shape((tiles, rows + 8, 2 * LANES)),
-        [VMEM] * 4,
+        [SMEM] + [VMEM] * 5,
         flops=2 * (rows + 8) * 2 * width * 2 * inner,
-        moved=own.size * 4,
-    )(arrived, affine, own, received)
+        moved=received.size * 4,
+    )(at, arrived, affine, gate_weight, up_weight, received)
     parts = lax.all_to_all(parts, "y", split_axis=0, concat_axis=0, tiled=True)
     hidden = call(functools.partial(activate_body, features), shape((tiles, rows, LANES)), [VMEM])(parts)
     hidden = lax.all_to_all(hidden, "y", split_axis=0, concat_axis=0, tiled=True)
@@ -260,7 +312,7 @@
     returned = lax.all_to_all(
         results.reshape(peers, 2 * SLOTS, LANES), ep, split_axis=0, concat_axis=0, tiled=True
     ).reshape(places, LANES)
-    return call(combine_body, shape((count, LANES)), [VMEM] * 4)(returned, groups, members, probs)
+    return call(combine_body, jax.ShapeDtypeStruct((count, LANES), bf16), [VMEM] * 2)(returned, weights)
 
 
 def solution(mesh):

time: 88.6 us -> 74.6 us (0.84)
  blocking collectives: 49.7 us -> 62.1 us
  waiting for transfers between devices: 7.8 us -> 0.01 us
  Pallas kernels: 11.1 us -> 3.41 us
  starting transfers between devices: 16.3 us -> 8.72 us
  local copies, waits for them, and re-layouts: 2.08 us -> 0.01 us
  other arithmetic: 0.89 us -> 0 us
    all_to_all x0 -> x1, blocking collectives: none -> 16 us  [on_device(): lax.all_to_all(outgoing.reshape(peers, 2 * SLOTS, LANES), ep, split_axis=...]
    all_to_all x1 -> x0, waiting for transfers between devices: 7.79 us -> none  [on_device(): lax.all_to_all(outgoing.reshape(peers, 2 * SLOTS, LANES), ep, split_axis=...]
    pallas_call x6, Pallas kernels: 11.1 us -> 3.41 us  [run(): return kernel(*near)]
    all_to_all x1 -> x0, starting transfers between devices: 7.58 us -> none  [on_device(): lax.all_to_all(outgoing.reshape(peers, 2 * SLOTS, LANES), ep, split_axis=...]
    all_to_all x1, blocking collectives: 13.8 us -> 11.8 us  [on_device(): lax.all_to_all(hidden, 'y', split_axis=0, concat_axis=0, tiled=True)]
    all_to_all x1, blocking collectives: 13.1 us -> 11.7 us  [on_device(): lax.all_to_all(results.reshape(peers, 2 * SLOTS, LANES), ep, split_axis=0...]
    dynamic_slice x1 -> x0, local copies, waits for them, and re-layouts: 1.28 us -> none  [on_device(): pick = lambda w, i: lax.dynamic_index_in_dim(w, i, 0, keepdims=False)]
    all_gather x1, blocking collectives: 3.06 us -> 1.82 us  [on_device(): both = lax.all_gather(mine, 'c', axis=0, tiled=False)]
  transfers between devices with their start and end apart: 2 -> 1, of which waited for: 1 -> 0; matrix products, arithmetic and copies ran while one was open for 1% -> 0% of each run, Pallas kernels for 3% -> 0%
where the time goes in v2:
time: 74.6 us; the launch traced here: 74.3 us
  blocking collectives  62.1 us (83%)
  starting transfers between devices  8.72 us (12%)
  Pallas kernels  3.41 us (5%)
    all_to_all x1, blocking collectives, on_device(): parts = lax.all_to_all(parts, 'y', split_axis=0, concat_axis=0, tiled=True)  16.3 us
    all_to_all x1, blocking collectives, on_device(): lax.all_to_all(outgoing.reshape(peers, 2 * SLOTS, LANES), ep, split_axis=...  16 us
    all_to_all x1, blocking collectives, on_device(): lax.all_to_all(hidden, 'y', split_axis=0, concat_axis=0, tiled=True)  11.8 us
    all_to_all x1, blocking collectives, on_device(): lax.all_to_all(results.reshape(peers, 2 * SLOTS, LANES), ep, split_axis=0...  11.7 us
    ppermute x1, starting transfers between devices, on_device(): received = lax.ppermute(sent, 'c', [(0, 1), (1, 0)])  8.72 us
    all_gather x1, blocking collectives, on_device(): hidden = lax.all_gather(hidden, 'c', axis=0, tiled=False)  4.55 us
    pallas_call x6, Pallas kernels, run(): return kernel(*near)  3.41 us
    all_gather x1, blocking collectives, on_device(): both = lax.all_gather(mine, 'c', axis=0, tiled=False)  1.82 us
  transfers between devices with their start and end apart: 1, of which 0 were waited for; matrix products, arithmetic and copies ran while one was open for 0% of the time, Pallas kernels for 0%

profile of v2, /device:TPU:1, one launch (start us, length us, event | category | flops | bytes accessed | tf_op | source)
XLA Modules:
  0.0 74.3 jit_solution(7167784692812152708)
XLA Ops:
  0.0 0.0 copy-start
  0.0 0.0 copy-start.1
  0.0 1.3 %shard_map.91 = (bf16[16,128]{1,0:T(8,128)(2,1)S(1)}, bf16[2,128,1024]{2,1,0:T(8,128)(2,1)S(1)}, bf16[128,16]{1,0:T(8,128)(2,1)S(1)}, f32[128,8]{1,0:T(8,128)S(1)}) custom-call(s32[1]{0:T(128)} %bitcast.core, bf16[8,128]{1,0:T(8,128)(2,1)} %tokens.1, f32[1,128]{1,0:T(1,128)} %bitcast.20, f32[1,128]{1,0:T(1,128)} %bitcast.21, s32[1,8]{1,0:T(1,128)} %bitcast.22, ...), custom_call_target="tpu_custom_call" | custom-call | tf_op jit(solution)/shard_map/pallas_call | solution.py:40
  1.3 8.7 %collective-permute-start = (bf16[2,128,1024]{2,1,0:T(8,128)(2,1)S(1)}, bf16[2,128,1024]{2,1,0:T(8,128)(2,1)S(1)}, u32[]{:S(2)}, u32[]{:S(2)}) collective-permute-start(bf16[2,128,1024]{2,1,0:T(8,128)(2,1)S(1)} %get-tuple-element.15), channel_id=1, source_target_pairs={{0,1},{1,0},{2,3},{3,2},{4,5},{5,4},{6,7},{7,6},{8,9},{9,8},{10,11... | collective-permute-start | bytes 1572872 | tf_op jit(solution)/shard_map/ppermute | solution.py:285
  10.0 1.8 %all-gather = bf16[32,128]{1,0:T(8,128)(2,1)S(1)} all-gather(bf16[16,128]{1,0:T(8,128)(2,1)S(1)} %get-tuple-element.11), channel_id=2, replica_groups=mesh['z'=8,'x'=4,'y'=8,'c'=2] {'c'}, dimensions={0}, use_global_device_ids=true | all-gather | bytes 12288 | tf_op jit(solution)/shard_map/all_gather | solution.py:286
  11.8 0.1 shard_map.92
  12.0 16.0 %all_to_all.20 = bf16[32,4,128]{2,1,0:T(4,128)(2,1)S(1)} all-to-all(bf16[32,4,128]{2,1,0:T(4,128)(2,1)S(1)} %bitcast.16), channel_id=1, replica_groups=mesh['z'=8,'x'=4,'y'=8,'c'=2] {'z','x'}, dimensions={0} | all-to-all | bytes 65536 | tf_op jit(solution)/shard_map/all_to_all | solution.py:290
  28.0 0.0 collective-permute-done.received
  28.0 0.0 copy-done
  28.0 0.0 copy-done.1
  28.0 0.5 shard_map.93
  28.5 16.3 %all_to_all.21.parts = bf16[8,72,256]{2,1,0:T(8,128)(2,1)S(1)} all-to-all(bf16[8,72,256]{2,1,0:T(8,128)(2,1)S(1)} %shard_map.93), channel_id=1, replica_groups=mesh['z'=8,'x'=4,'y'=8,'c'=2] {'y'}, dimensions={0} | all-to-all | bytes 589824 | tf_op jit(solution)/shard_map/all_to_all | solution.py:301
  44.8 0.0 copy-start.2
  44.8 0.3 shard_map.94
  45.1 11.8 %all_to_all.22 = bf16[8,64,128]{2,1,0:T(8,128)(2,1)S(1)} all-to-all(bf16[8,64,128]{2,1,0:T(8,128)(2,1)S(1)} %shard_map.94), channel_id=1, replica_groups=mesh['z'=8,'x'=4,'y'=8,'c'=2] {'y'}, dimensions={0} | all-to-all | bytes 262144 | tf_op jit(solution)/shard_map/all_to_all | solution.py:303
  57.0 4.5 %all-gather.1 = bf16[16,64,128]{2,1,0:T(8,128)(2,1)S(1)} all-gather(bf16[8,64,128]{2,1,0:T(8,128)(2,1)S(1)} %all_to_all.22), channel_id=3, replica_groups=mesh['z'=8,'x'=4,'y'=8,'c'=2] {'c'}, dimensions={0}, use_global_device_ids=true | all-gather | bytes 393216 | tf_op jit(solution)/shard_map/all_gather | solution.py:304
  61.5 0.0 copy-done.2
  61.5 0.4 shard_map.95
  61.9 11.7 %all_to_all.23 = bf16[32,4,128]{2,1,0:T(4,128)(2,1)S(1)} all-to-all(bf16[32,4,128]{2,1,0:T(4,128)(2,1)S(1)} %bitcast.15), channel_id=1, replica_groups=mesh['z'=8,'x'=4,'y'=8,'c'=2] {'z','x'}, dimensions={0} | all-to-all | bytes 65536 | tf_op jit(solution)/shard_map/all_to_all | solution.py:312
  73.6 0.8 %shard_map.96 = bf16[8,128]{1,0:T(8,128)(2,1)} custom-call(bf16[128,128]{1,0:T(8,128)(2,1)S(1)} %bitcast.14, f32[128,8]{1,0:T(8,128)S(1)} %get-tuple-element.16.weights), custom_call_target="tpu_custom_call" | custom-call | tf_op jit(solution)/shard_map/pallas_call | solution.py:40
Async XLA Ops:
  0.0 28.0 %copy-start = (bf16[2,128,1024]{2,1,0:T(8,128)(2,1)S(1)}, bf16[2,128,1024]{2,1,0:T(8,128)(2,1)}, u32[]{:S(2)}) copy-start(bf16[2,128,1024]{2,1,0:T(8,128)(2,1)} %gate.3) | copy-start | bytes 1572868
  0.0 28.0 %copy-start.1 = (bf16[2,128,1024]{2,1,0:T(8,128)(2,1)S(1)}, bf16[2,128,1024]{2,1,0:T(8,128)(2,1)}, u32[]{:S(2)}) copy-start(bf16[2,128,1024]{2,1,0:T(8,128)(2,1)} %up.3) | copy-start | bytes 1572868
  1.3 26.7 %collective-permute-start = (bf16[2,128,1024]{2,1,0:T(8,128)(2,1)S(1)}, bf16[2,128,1024]{2,1,0:T(8,128)(2,1)S(1)}, u32[]{:S(2)}, u32[]{:S(2)}) collective-permute-start(bf16[2,128,1024]{2,1,0:T(8,128)(2,1)S(1)} %get-tuple-element.15), channel_id=1, source_target_pairs={{0,1},{1,0},{2,3},{3,2},{4,5},{5,4},{6,7},{7,6},{8,9},{9,8},{10,11... | collective-permute-start | bytes 1572872 | tf_op jit(solution)/shard_map/ppermute | solution.py:285
  44.8 16.7 %copy-start.2 = (bf16[2,1024,128]{2,1,0:T(8,128)(2,1)S(1)}, bf16[2,1024,128]{2,1,0:T(8,128)(2,1)}, u32[]{:S(2)}) copy-start(bf16[2,1024,128]{2,1,0:T(8,128)(2,1)} %down.1) | copy-start | bytes 1572868

commit v3 on v2

--- a/solution.py
+++ b/solution.py
@@ -7,6 +7,7 @@
 from jax.experimental.pallas import tpu as pltpu
 from jax.sharding import Mesh
 from jax.sharding import PartitionSpec as P
+
 
 f32 = jnp.float32
 bf16 = jnp.bfloat16
@@ -79,9 +80,20 @@
     return slots
 
 
-def share_body(core, tokens, gain, bias, groups, members, probs, gate, up, out, sent, hits, weights, *scratch):
+def slice_body(core, gate, up, sent, arrived):
+    peer = 1 - core[0]
+    copies = [
+        pltpu.make_async_copy(gate.at[peer], sent.at[0], arrived.at[0]),
+        pltpu.make_async_copy(up.at[peer], sent.at[1], arrived.at[1]),
+    ]
+    for copy in copies:
+        copy.start()
+    for copy in copies:
+        copy.wait()
+
+
+def share_body(tokens, gain, bias, groups, members, probs, out, hits, weights, *scratch):
     near_gain, near_bias, near_groups, near_members, near_probs, arrived = scratch
-    peer = 1 - core[0]
     pairs = (
         (gain, near_gain),
         (bias, near_bias),
@@ -89,8 +101,6 @@
         (members, near_members),
         (probs, near_probs),
         (tokens, out.at[0:8]),
-        (gate.at[peer], sent.at[0]),
-        (up.at[peer], sent.at[1]),
     )
     copies = [pltpu.make_async_copy(a, b, arrived.at[i]) for i, (a, b) in enumerate(pairs)]
     for copy in copies:
@@ -209,7 +219,7 @@
 
 
 def project_body(hidden, down, out):
-    experts, tiles, rows, width = hidden.shape
+    experts, tiles, rows, _ = hidden.shape
     places = out.shape[0]
     row, source = iota((places, rows), 0), iota((places, rows), 1)
     total = jnp.zeros((places, LANES), f32)
@@ -254,42 +264,42 @@
     groups, members, probs = group_pick.T, member_pick.T, picked_probs.T
 
     at = core.reshape(1)
-    mine, sent, hits, weights = call(
+    mine, hits, weights = call(
         share_body,
-        (
-            shape((16, LANES)),
-            shape((2, width, inner)),
-            shape((places, 2 * count)),
-            shape((places, count), f32),
-        ),
-        [SMEM] + [ANY] * 8,
+        (shape((16, LANES)), shape((places, 2 * count)), shape((places, count), f32)),
+        [ANY] * 6,
         scratch=[
             pltpu.VMEM((1, width), f32),
             pltpu.VMEM((1, width), f32),
             pltpu.VMEM(groups.shape, groups.dtype),
             pltpu.VMEM(members.shape, members.dtype),
             pltpu.VMEM(probs.shape, probs.dtype),
-            pltpu.SemaphoreType.DMA((8,)),
+            pltpu.SemaphoreType.DMA((6,)),
         ],
     )(
-        at,
         tokens,
         norm_gain.reshape(1, width),
         norm_bias.reshape(1, width),
         groups,
         members,
         probs,
-        gate_weight,
-        up_weight,
-    )
+    )
+    sent = call(
+        slice_body,
+        shape((2, width, inner)),
+        [SMEM, ANY, ANY],
+        flops=1 << 20,
+        moved=2 * width * inner * 2,
+        scratch=[pltpu.SemaphoreType.DMA((2,))],
+    )(at, gate_weight, up_weight)
     received = lax.ppermute(sent, "c", [(0, 1), (1, 0)])
     both = lax.all_gather(mine, "c", axis=0, tiled=False)
     outgoing, affine = call(
         pack_body, (shape((places, LANES)), shape((8, 2 * LANES))), [SMEM] + [VMEM] * 2
     )(at, both, hits)
-    arrived = lax.all_to_all(
-        outgoing.reshape(peers, 2 * SLOTS, LANES), ep, split_axis=0, concat_axis=0, tiled=True
-    ).reshape(places, LANES)
+    outgoing = outgoing.reshape(peers, 2 * SLOTS, LANES)
+    arrived = lax.all_to_all(outgoing, ep, split_axis=0, concat_axis=0, tiled=True)
+    arrived = arrived.reshape(places, LANES)
 
     parts = call(
         spread_body,

time: 74.6 us -> 76.2 us (1.021)
  Pallas kernels: 3.41 us -> 4.23 us
    all_to_all x1, blocking collectives: 11.8 us -> 11 us  [on_device(): lax.all_to_all(hidden, 'y', split_axis=0, concat_axis=0, tiled=True)]
    pallas_call x6 -> x7, Pallas kernels: 3.41 us -> 4.23 us  [run(): return kernel(*near)]
    all_to_all x1, blocking collectives: 16.3 us -> 17.1 us  [on_device(): parts = lax.all_to_all(parts, 'y', split_axis=0, concat_axis=0, tiled=True)]
  transfers between devices with their start and end apart: 1 -> 1, of which waited for: 0 -> 0; matrix products, arithmetic and copies ran while one was open for 0% -> 0% of each run, Pallas kernels for 0% -> 1%
where the time goes in v3:
time: 76.2 us; the launch traced here: 75.8 us
  blocking collectives  62.8 us (82%)
  starting transfers between devices  8.75 us (11%)
  Pallas kernels  4.23 us (6%)
    all_to_all x1, blocking collectives, on_device(): parts = lax.all_to_all(parts, 'y', split_axis=0, concat_axis=0, tiled=True)  17.1 us
    all_to_all x1, blocking collectives, on_device(): lax.all_to_all(outgoing, ep, split_axis=0, concat_axis=0, tiled=True)  16.1 us
    all_to_all x1, blocking collectives, on_device(): lax.all_to_all(results.reshape(peers, 2 * SLOTS, LANES), ep, split_axis=0...  11.6 us
    all_to_all x1, blocking collectives, on_device(): lax.all_to_all(hidden, 'y', split_axis=0, concat_axis=0, tiled=True)  11 us
    ppermute x1, starting transfers between devices, on_device(): received = lax.ppermute(sent, 'c', [(0, 1), (1, 0)])  8.75 us
    all_gather x1, blocking collectives, on_device(): hidden = lax.all_gather(hidden, 'c', axis=0, tiled=False)  5.19 us
    pallas_call x7, Pallas kernels, run(): return kernel(*near)  4.23 us
    all_gather x1, blocking collectives, on_device(): both = lax.all_gather(mine, 'c', axis=0, tiled=False)  1.82 us
  transfers between devices with their start and end apart: 1, of which 0 were waited for; matrix products, arithmetic and copies ran while one was open for 0% of the time, Pallas kernels for 1%

profile of v3, /device:TPU:1, one launch (start us, length us, event | category | flops | bytes accessed | tf_op | source)
XLA Modules:
  0.0 75.8 jit_solution(12995877487856647896)
XLA Ops:
  0.0 0.0 copy-start
  0.0 0.0 copy-start.1
  0.0 1.1 %shard_map.93 = bf16[2,128,1024]{2,1,0:T(8,128)(2,1)S(1)} custom-call(s32[1]{0:T(128)} %bitcast.core, bf16[2,128,1024]{2,1,0:T(8,128)(2,1)} %gate.3, bf16[2,128,1024]{2,1,0:T(8,128)(2,1)} %up.3), custom_call_target="tpu_custom_call" | custom-call | flops 1048576 | bytes 524288 | tf_op jit(solution)/shard_map/pallas_call | solution.py:41
  1.1 8.7 %collective-permute-start = (bf16[2,128,1024]{2,1,0:T(8,128)(2,1)S(1)}, bf16[2,128,1024]{2,1,0:T(8,128)(2,1)S(1)}, u32[]{:S(2)}, u32[]{:S(2)}) collective-permute-start(bf16[2,128,1024]{2,1,0:T(8,128)(2,1)S(1)} %shard_map.93), channel_id=1, source_target_pairs={{0,1},{1,0},{2,3},{3,2},{4,5},{5,4},{6,7},{7,6},{8,9},{9,8},{10,11... | collective-permute-start | bytes 1572872 | tf_op jit(solution)/shard_map/ppermute | solution.py:295
  9.9 1.0 %shard_map.91 = (bf16[16,128]{1,0:T(8,128)(2,1)S(1)}, bf16[128,16]{1,0:T(8,128)(2,1)S(1)}, f32[128,8]{1,0:T(8,128)S(1)}) custom-call(bf16[8,128]{1,0:T(8,128)(2,1)} %tokens.1, f32[1,128]{1,0:T(1,128)} %bitcast.20, f32[1,128]{1,0:T(1,128)} %bitcast.21, s32[1,8]{1,0:T(1,128)} %bitcast.22, s32[4,8]{1,0:T(4,128)} %bitcast.18, f32[4,8]{1,0:T(4,128)} %bitcast.19), custom_call_target="tpu_custom_call" | custom-call | tf_op jit(solution)/shard_map/pallas_call | solution.py:41
  10.9 1.8 %all-gather = bf16[32,128]{1,0:T(8,128)(2,1)S(1)} all-gather(bf16[16,128]{1,0:T(8,128)(2,1)S(1)} %get-tuple-element.10), channel_id=2, replica_groups=mesh['z'=8,'x'=4,'y'=8,'c'=2] {'c'}, dimensions={0}, use_global_device_ids=true | all-gather | bytes 12288 | tf_op jit(solution)/shard_map/all_gather | solution.py:296
  12.7 0.1 shard_map.92
  12.8 16.1 %all_to_all.20 = bf16[32,4,128]{2,1,0:T(4,128)(2,1)S(1)} all-to-all(bf16[32,4,128]{2,1,0:T(4,128)(2,1)S(1)} %bitcast.16), channel_id=1, replica_groups=mesh['z'=8,'x'=4,'y'=8,'c'=2] {'z','x'}, dimensions={0} | all-to-all | bytes 65536 | tf_op jit(solution)/shard_map/all_to_all | solution.py:301
  28.9 0.0 collective-permute-done.received
  29.0 0.0 copy-done
  29.0 0.0 copy-done.1
  29.0 0.5 shard_map.94
  29.5 17.1 %all_to_all.21.parts = bf16[8,72,256]{2,1,0:T(8,128)(2,1)S(1)} all-to-all(bf16[8,72,256]{2,1,0:T(8,128)(2,1)S(1)} %shard_map.94), channel_id=1, replica_groups=mesh['z'=8,'x'=4,'y'=8,'c'=2] {'y'}, dimensions={0} | all-to-all | bytes 589824 | tf_op jit(solution)/shard_map/all_to_all | solution.py:311
  46.6 0.0 copy-start.2
  46.6 0.3 shard_map.95
  46.9 11.0 %all_to_all.22 = bf16[8,64,128]{2,1,0:T(8,128)(2,1)S(1)} all-to-all(bf16[8,64,128]{2,1,0:T(8,128)(2,1)S(1)} %shard_map.95), channel_id=1, replica_groups=mesh['z'=8,'x'=4,'y'=8,'c'=2] {'y'}, dimensions={0} | all-to-all | bytes 262144 | tf_op jit(solution)/shard_map/all_to_all | solution.py:313
  57.9 5.2 %all-gather.1 = bf16[16,64,128]{2,1,0:T(8,128)(2,1)S(1)} all-gather(bf16[8,64,128]{2,1,0:T(8,128)(2,1)S(1)} %all_to_all.22), channel_id=3, replica_groups=mesh['z'=8,'x'=4,'y'=8,'c'=2] {'c'}, dimensions={0}, use_global_device_ids=true | all-gather | bytes 393216 | tf_op jit(solution)/shard_map/all_gather | solution.py:314
  63.1 0.0 copy-done.2
  63.1 0.4 shard_map.96
  63.5 11.6 %all_to_all.23 = bf16[32,4,128]{2,1,0:T(4,128)(2,1)S(1)} all-to-all(bf16[32,4,128]{2,1,0:T(4,128)(2,1)S(1)} %bitcast.15), channel_id=1, replica_groups=mesh['z'=8,'x'=4,'y'=8,'c'=2] {'z','x'}, dimensions={0} | all-to-all | bytes 65536 | tf_op jit(solution)/shard_map/all_to_all | solution.py:322
  75.1 0.8 %shard_map.97 = bf16[8,128]{1,0:T(8,128)(2,1)} custom-call(bf16[128,128]{1,0:T(8,128)(2,1)S(1)} %bitcast.14, f32[128,8]{1,0:T(8,128)S(1)} %get-tuple-element.14.weights), custom_call_target="tpu_custom_call" | custom-call | tf_op jit(solution)/shard_map/pallas_call | solution.py:41
Async XLA Ops:
  0.0 29.0 %copy-start = (bf16[2,128,1024]{2,1,0:T(8,128)(2,1)S(1)}, bf16[2,128,1024]{2,1,0:T(8,128)(2,1)}, u32[]{:S(2)}) copy-start(bf16[2,128,1024]{2,1,0:T(8,128)(2,1)} %gate.3) | copy-start | bytes 1572868
  0.0 29.0 %copy-start.1 = (bf16[2,128,1024]{2,1,0:T(8,128)(2,1)S(1)}, bf16[2,128,1024]{2,1,0:T(8,128)(2,1)}, u32[]{:S(2)}) copy-start(bf16[2,128,1024]{2,1,0:T(8,128)(2,1)} %up.3) | copy-start | bytes 1572868
  1.1 27.8 %collective-permute-start = (bf16[2,128,1024]{2,1,0:T(8,128)(2,1)S(1)}, bf16[2,128,1024]{2,1,0:T(8,128)(2,1)S(1)}, u32[]{:S(2)}, u32[]{:S(2)}) collective-permute-start(bf16[2,128,1024]{2,1,0:T(8,128)(2,1)S(1)} %shard_map.93), channel_id=1, source_target_pairs={{0,1},{1,0},{2,3},{3,2},{4,5},{5,4},{6,7},{7,6},{8,9},{9,8},{10,11... | collective-permute-start | bytes 1572872 | tf_op jit(solution)/shard_map/ppermute | solution.py:295
  46.6 16.5 %copy-start.2 = (bf16[2,1024,128]{2,1,0:T(8,128)(2,1)S(1)}, bf16[2,1024,128]{2,1,0:T(8,128)(2,1)}, u32[]{:S(2)}) copy-start(bf16[2,1024,128]{2,1,0:T(8,128)(2,1)} %down.1) | copy-start | bytes 1572868

commit v4 on v2

--- a/solution.py
+++ b/solution.py
@@ -79,41 +79,33 @@
     return slots
 
 
-def share_body(core, tokens, gain, bias, groups, members, probs, gate, up, out, sent, hits, weights, *scratch):
-    near_gain, near_bias, near_groups, near_members, near_probs, arrived = scratch
-    peer = 1 - core[0]
+def place_body(core, tokens, groups, members, probs, gain, bias, gate, up, out, weights, affine, *scratch):
+    near_tokens, near_groups, near_members, near_probs, near_gain, near_bias, arrived = scratch
     pairs = (
+        (groups, near_groups),
+        (tokens, near_tokens),
+        (members, near_members),
+        (probs, near_probs),
         (gain, near_gain),
         (bias, near_bias),
-        (groups, near_groups),
-        (members, near_members),
-        (probs, near_probs),
-        (tokens, out.at[0:8]),
-        (gate.at[peer], sent.at[0]),
-        (up.at[peer], sent.at[1]),
     )
     copies = [pltpu.make_async_copy(a, b, arrived.at[i]) for i, (a, b) in enumerate(pairs)]
     for copy in copies:
         copy.start()
-    for copy in copies[0:5]:
+    for copy in copies:
         copy.wait()
-    rows = three(near_gain[...]) + three(near_bias[...])
-    out[8:16, :] = by_row(rows, LANES).astype(bf16)
-
-    place = hits.shape[0]
+    place = out.shape[0]
     per = place // 8
     chosen = near_groups[...]
     slots = slots_of(chosen)
-    pair = jnp.concatenate([chosen, chosen], axis=1)
-    slot_pair = jnp.concatenate([slots, slots], axis=1)
+    none = jnp.full((1, 8), -1, jnp.int32)
+    pair = jnp.concatenate([chosen, none], axis=1)
+    slot_pair = jnp.concatenate([slots, none], axis=1)
     row = iota((place, 16), 0)
-    half = jnp.where(iota((place, 16), 1) >= 8, 1, 0)
-    hit = (
-        (row // per == pair)
-        & (row % SLOTS == slot_pair)
-        & ((row // SLOTS) % 2 == half)
-    )
-    hits[...] = jnp.where(hit, 1.0, 0.0).astype(bf16)
+    hit = (row // per == pair) & (row % (2 * SLOTS) == slot_pair)
+    values = near_tokens[...].astype(f32)
+    values = jnp.concatenate([values, jnp.zeros_like(values)], axis=0).astype(bf16)
+    out[...] = dot(jnp.where(hit, 1.0, 0.0).astype(bf16), values).astype(bf16)
 
     likely = near_probs[...]
     shares = likely / jnp.sum(likely, axis=0, keepdims=True)
@@ -123,62 +115,70 @@
         member = near_members[k : k + 1, :]
         at = (chosen * (EPG // 2) + member // 2) * (2 * SLOTS) + (member % 2) * SLOTS + slots
         total = total + jnp.where(row == at, shares[k : k + 1, :], 0.0)
-    weights[...] = total
-    for copy in copies[5:]:
-        copy.wait()
-
-
-def pack_body(core, both, hits, out, affine):
-    first, second = both[0].astype(f32), both[1].astype(f32)
-    lower = core[0] == 0
-    own, other = jnp.where(lower, first, second), jnp.where(lower, second, first)
-    affine[:, 0:LANES] = own[8:16].astype(bf16)
-    affine[:, LANES:] = other[8:16].astype(bf16)
-    values = jnp.concatenate([own[0:8], other[0:8]], axis=0).astype(bf16)
-    out[...] = dot(hits[...], values).astype(bf16)
-
-
-def spread_body(core, arrived, affine, gate, up, received, out):
+    weights[...] = jnp.concatenate(three(total), axis=1).astype(bf16)
+    affine[...] = by_row(three(near_gain[...]) + three(near_bias[...]), LANES).astype(bf16)
+
+
+def spread_body(core, arrived, affine, gate, up, kept, given):
     places = arrived.shape[0]
     rows = places // 2
     at, source = iota((rows, places), 0), iota((rows, places), 1)
-    values = arrived[...]
-    halves = []
-    for half in range(2):
-        takes = source == (at // SLOTS) * (2 * SLOTS) + half * SLOTS + at % SLOTS
-        halves.append(dot(jnp.where(takes, 1.0, 0.0).astype(bf16), values))
-    features = 2 * LANES
-    mean = (
-        jnp.sum(halves[0], axis=1, keepdims=True) + jnp.sum(halves[1], axis=1, keepdims=True)
-    ) / features
-    centred = [h - mean for h in halves]
-    square = jnp.sum(centred[0] * centred[0] + centred[1] * centred[1], axis=1, keepdims=True)
+    takes = source == (at // SLOTS) * (2 * SLOTS) + at % SLOTS
+    values = dot(jnp.where(takes, 1.0, 0.0).astype(bf16), arrived[...])
+    mean = jnp.sum(values, axis=1, keepdims=True) / LANES
+    centred = values - mean
+    square = jnp.sum(centred * centred, axis=1, keepdims=True)
 
     lane = iota((rows, LANES), 1)
     stats = jnp.where(lane == 0, mean, jnp.where(lane == 1, square, 0.0))
     stats = jnp.concatenate([stats, jnp.zeros((LANES - rows, LANES), f32)], axis=0).T
-    means, squares = three(stats[0:1]), three(stats[1:2])
-
-    left = []
-    for half in range(2):
-        lanes = slice(half * LANES, (half + 1) * LANES)
-        affine_rows = affine[:, lanes]
-        wide = affine_rows.astype(f32)
-        gain = wide[0:1] + wide[1:2] + wide[2:3]
-        left.append(jnp.concatenate([(centred[half] * gain).astype(bf16), affine_rows], axis=0))
-
-    for mat, stat in ((0, means), (1, squares)):
-        own = (gate, up)[mat][core[0]]
-        total = dot(left[0], own) + dot(left[1], received[mat])
-        tail = total[rows : rows + 8]
-        gain_sum = tail[0:1] + tail[1:2] + tail[2:3]
-        bias_sum = tail[3:4] + tail[4:5] + tail[5:6]
-        parts = three(gain_sum)[0:2] + three(bias_sum)[0:2]
-        for y in range(out.shape[0]):
-            lanes = slice(y * LANES, (y + 1) * LANES)
+
+    wide = affine[...].astype(f32)
+    gain = wide[0:1] + wide[1:2] + wide[2:3]
+    left = jnp.concatenate([(centred * gain).astype(bf16), affine[...]], axis=0)
+    none = jnp.zeros((1, LANES), f32)
+    for out, expert in ((kept, core[0]), (given, 1 - core[0])):
+        split = out is given
+        for mat, weight in enumerate((gate, up)):
+            total = dot(left, weight[expert])
+            tail = total[rows : rows + 8]
+            gain_sum = tail[0:1] + tail[1:2] + tail[2:3]
+            bias_sum = tail[3:4] + tail[4:5] + tail[5:6]
+            stat = stats[mat : mat + 1]
             put = slice(mat * LANES, (mat + 1) * LANES)
-            out[y, 0:rows, put] = total[0:rows, lanes].astype(bf16)
-            out[y, rows : rows + 8, put] = by_row([p[:, lanes] for p in parts] + list(stat), LANES).astype(bf16)
+            for y in range(out.shape[0]):
+                lanes = slice(y * LANES, (y + 1) * LANES)
+                out[y, 0:rows, put] = total[0:rows, lanes].astype(out.dtype)
+                g, b = gain_sum[:, lanes], bias_sum[:, lanes]
+                parts = three(g)[0:2] + three(b)[0:2] + three(stat) if split else (g, none, b, none, stat)
+                out[y, rows : rows + 8, put] = by_row(parts, LANES).astype(out.dtype)
+
+
+def merge_body(width, core, kept, both, out):
+    tiles, tall, wide = kept.shape
+    rows = tall - 8
+    peer = 1 - core[0]
+    mine, theirs = kept[0, rows:tall, :], both[peer, 0, rows:tall, :].astype(f32)
+    theirs = theirs[4:5] + theirs[5:6] + theirs[6:7]
+    own_mean, own_square = mine[4:5, 0:LANES], mine[4:5, LANES:]
+    other_mean, other_square = theirs[:, 0:LANES], theirs[:, LANES:]
+    mean = (own_mean + other_mean) * 0.5
+    own_shift, other_shift = own_mean - mean, other_mean - mean
+    square = own_square + other_square + width * (own_shift * own_shift + other_shift * other_shift)
+    stats = three(jnp.concatenate([mean, square], axis=1))
+    turned = jnp.concatenate(
+        [by_row([own_shift, other_shift], LANES), jnp.zeros((LANES - 8, LANES), f32)], axis=0
+    ).T
+    own_shift, other_shift = turned[0:rows, 0:1], turned[0:rows, 1:2]
+    for y in range(tiles):
+        own_tail, other_tail = kept[y, rows:tall, :], both[peer, y, rows:tall, :].astype(f32)
+        own_gain, other_gain = own_tail[0:1], other_tail[0:1] + other_tail[1:2]
+        bias = own_tail[2:3] + other_tail[2:3] + other_tail[3:4]
+        total = kept[y, 0:rows, :] + both[peer, y, 0:rows, :].astype(f32)
+        total = total + own_shift * own_gain + other_shift * other_gain
+        out[y, 0:rows, :] = total.astype(bf16)
+        parts = three(own_gain + other_gain)[0:2] + three(bias)[0:2] + stats
+        out[y, rows:tall, :] = by_row(parts, wide).astype(bf16)
 
 
 def activate_body(features, parts, out):
@@ -222,12 +222,11 @@
 
 
 def combine_body(returned, weights, out):
-    values = returned[...]
-    total = jnp.zeros(out.shape, f32)
-    for part in three(weights[...]):
-        total = total + lax.dot_general(
-            part.astype(bf16), values, (((0,), (0,)), ((), ())), preferred_element_type=f32
-        )
+    count = out.shape[0]
+    total = lax.dot_general(
+        weights[...], returned[...], (((0,), (0,)), ((), ())), preferred_element_type=f32
+    )
+    total = total[0:count] + total[count : 2 * count] + total[2 * count :]
     out[...] = total.astype(bf16)
 
 
@@ -254,50 +253,44 @@
     groups, members, probs = group_pick.T, member_pick.T, picked_probs.T
 
     at = core.reshape(1)
-    mine, sent, hits, weights = call(
-        share_body,
-        (
-            shape((16, LANES)),
-            shape((2, width, inner)),
-            shape((places, 2 * count)),
-            shape((places, count), f32),
-        ),
+    outgoing, weights, affine = call(
+        place_body,
+        (shape((places, LANES)), shape((places, 3 * count)), shape((8, LANES))),
         [SMEM] + [ANY] * 8,
         scratch=[
-            pltpu.VMEM((1, width), f32),
-            pltpu.VMEM((1, width), f32),
+            pltpu.VMEM(tokens.shape, tokens.dtype),
             pltpu.VMEM(groups.shape, groups.dtype),
             pltpu.VMEM(members.shape, members.dtype),
             pltpu.VMEM(probs.shape, probs.dtype),
-            pltpu.SemaphoreType.DMA((8,)),
+            pltpu.VMEM((1, width), f32),
+            pltpu.VMEM((1, width), f32),
+            pltpu.SemaphoreType.DMA((6,)),
         ],
     )(
         at,
         tokens,
-        norm_gain.reshape(1, width),
-        norm_bias.reshape(1, width),
         groups,
         members,
         probs,
+        norm_gain.reshape(1, width),
+        norm_bias.reshape(1, width),
         gate_weight,
         up_weight,
     )
-    received = lax.ppermute(sent, "c", [(0, 1), (1, 0)])
-    both = lax.all_gather(mine, "c", axis=0, tiled=False)
-    outgoing, affine = call(
-        pack_body, (shape((places, LANES)), shape((8, 2 * LANES))), [SMEM] + [VMEM] * 2
-    )(at, both, hits)
     arrived = lax.all_to_all(
         outgoing.reshape(peers, 2 * SLOTS, LANES), ep, split_axis=0, concat_axis=0, tiled=True
     ).reshape(places, LANES)
 
-    parts = call(
+    whole = (tiles, rows + 8, 2 * LANES)
+    kept, given = call(
         spread_body,
-        shape((tiles, rows + 8, 2 * LANES)),
-        [SMEM] + [VMEM] * 5,
-        flops=2 * (rows + 8) * 2 * width * 2 * inner,
-        moved=received.size * 4,
-    )(at, arrived, affine, gate_weight, up_weight, received)
+        (shape(whole, f32), shape(whole)),
+        [SMEM] + [VMEM] * 4,
+        flops=2 * (rows + 8) * width * 4 * inner,
+        moved=gate_weight.size * 4,
+    )(at, arrived, affine, gate_weight, up_weight)
+    both = lax.all_gather(given, "c", axis=0, tiled=False)
+    parts = call(functools.partial(merge_body, width), shape(whole), [SMEM] + [VMEM] * 2)(at, kept, both)
     parts = lax.all_to_all(parts, "y", split_axis=0, concat_axis=0, tiled=True)
     hidden = call(functools.partial(activate_body, features), shape((tiles, rows, LANES)), [VMEM])(parts)
     hidden = lax.all_to_all(hidden, "y", split_axis=0, concat_axis=0, tiled=True)

time: 74.6 us -> 73.9 us (level)
  starting transfers between devices: 8.72 us -> 0 us
  blocking collectives: 62.1 us -> 70.3 us
    ppermute x1 -> x0, starting transfers between devices: 8.72 us -> none  [on_device(): received = lax.ppermute(sent, 'c', [(0, 1), (1, 0)])]
    all_to_all x1, blocking collectives: 16 us -> 22.1 us  [on_device(): lax.all_to_all(outgoing.reshape(peers, 2 * SLOTS, LANES), ep, split_axis=...]
    all_gather x1, blocking collectives: 1.82 us -> 3.96 us  [on_device(): both = lax.all_gather(given, 'c', axis=0, tiled=False)]
    all_to_all x1, blocking collectives: 16.3 us -> 18 us  [on_device(): parts = lax.all_to_all(parts, 'y', split_axis=0, concat_axis=0, tiled=True)]
    all_to_all x1, blocking collectives: 11.8 us -> 10.1 us  [on_device(): lax.all_to_all(hidden, 'y', split_axis=0, concat_axis=0, tiled=True)]
  transfers between devices with their start and end apart: 1 -> 0, of which waited for: 0 -> 0; matrix products, arithmetic and copies ran while one was open for 0% -> 0% of each run, Pallas kernels for 0% -> 0%
where the time goes in v4:
time: 73.9 us; the launch traced here: 73.7 us
  blocking collectives  70.3 us (95%)
  Pallas kernels  3.32 us (4%)
    all_to_all x1, blocking collectives, on_device(): lax.all_to_all(outgoing.reshape(peers, 2 * SLOTS, LANES), ep, split_axis=...  22.1 us
    all_to_all x1, blocking collectives, on_device(): parts = lax.all_to_all(parts, 'y', split_axis=0, concat_axis=0, tiled=True)  18 us
    all_to_all x1, blocking collectives, on_device(): lax.all_to_all(results.reshape(peers, 2 * SLOTS, LANES), ep, split_axis=0...  11.6 us
    all_to_all x1, blocking collectives, on_device(): lax.all_to_all(hidden, 'y', split_axis=0, concat_axis=0, tiled=True)  10.1 us
    all_gather x1, blocking collectives, on_device(): hidden = lax.all_gather(hidden, 'c', axis=0, tiled=False)  4.42 us
    all_gather x1, blocking collectives, on_device(): both = lax.all_gather(given, 'c', axis=0, tiled=False)  3.96 us
    pallas_call x6, Pallas kernels, run(): return kernel(*near)  3.32 us

profile of v4, /device:TPU:1, one launch (start us, length us, event | category | flops | bytes accessed | tf_op | source)
XLA Modules:
  0.0 73.7 jit_solution(4681365499180890710)
XLA Ops:
  0.0 0.0 copy-start
  0.0 0.0 copy-start.1
  0.0 1.1 %shard_map.91 = (bf16[128,128]{1,0:T(8,128)(2,1)S(1)}, bf16[128,24]{1,0:T(8,128)(2,1)S(1)}, bf16[8,128]{1,0:T(8,128)(2,1)S(1)}) custom-call(s32[1]{0:T(128)} %bitcast.core, bf16[8,128]{1,0:T(8,128)(2,1)} %tokens.1, s32[1,8]{1,0:T(1,128)} %bitcast.20, s32[4,8]{1,0:T(4,128)} %bitcast.18, f32[4,8]{1,0:T(4,128)} %bitcast.19, f32[1,128]{1,0:T(1,128)} %bitcast.21, ...), custom_call_target="tpu_custom_call" | custom-call | tf_op jit(solution)/shard_map/pallas_call | solution.py:40
  1.1 22.1 %all_to_all.20 = bf16[32,4,128]{2,1,0:T(4,128)(2,1)S(1)} all-to-all(bf16[32,4,128]{2,1,0:T(4,128)(2,1)S(1)} %bitcast.17), channel_id=1, replica_groups=mesh['z'=8,'x'=4,'y'=8,'c'=2] {'z','x'}, dimensions={0} | all-to-all | bytes 65536 | tf_op jit(solution)/shard_map/all_to_all | solution.py:280
  23.3 0.0 copy-done
  23.3 0.0 copy-done.1
  23.3 0.5 shard_map.92
  23.8 4.0 %all-gather = bf16[16,72,256]{2,1,0:T(8,128)(2,1)S(1)} all-gather(bf16[8,72,256]{2,1,0:T(8,128)(2,1)S(1)} %get-tuple-element.13), channel_id=2, replica_groups=mesh['z'=8,'x'=4,'y'=8,'c'=2] {'c'}, dimensions={0}, use_global_device_ids=true | all-gather | bytes 884736 | tf_op jit(solution)/shard_map/all_gather | solution.py:292
  27.8 0.2 shard_map.93
  28.0 18.0 %all_to_all.21.parts = bf16[8,72,256]{2,1,0:T(8,128)(2,1)S(1)} all-to-all(bf16[8,72,256]{2,1,0:T(8,128)(2,1)S(1)} %shard_map.93), channel_id=1, replica_groups=mesh['z'=8,'x'=4,'y'=8,'c'=2] {'y'}, dimensions={0} | all-to-all | bytes 589824 | tf_op jit(solution)/shard_map/all_to_all | solution.py:294
  46.0 0.0 copy-start.2
  46.0 0.3 shard_map.94
  46.4 10.1 %all_to_all.22 = bf16[8,64,128]{2,1,0:T(8,128)(2,1)S(1)} all-to-all(bf16[8,64,128]{2,1,0:T(8,128)(2,1)S(1)} %shard_map.94), channel_id=1, replica_groups=mesh['z'=8,'x'=4,'y'=8,'c'=2] {'y'}, dimensions={0} | all-to-all | bytes 262144 | tf_op jit(solution)/shard_map/all_to_all | solution.py:296
  56.5 4.4 %all-gather.1 = bf16[16,64,128]{2,1,0:T(8,128)(2,1)S(1)} all-gather(bf16[8,64,128]{2,1,0:T(8,128)(2,1)S(1)} %all_to_all.22), channel_id=3, replica_groups=mesh['z'=8,'x'=4,'y'=8,'c'=2] {'c'}, dimensions={0}, use_global_device_ids=true | all-gather | bytes 393216 | tf_op jit(solution)/shard_map/all_gather | solution.py:297
  60.9 0.0 copy-done.2
  60.9 0.4 shard_map.95
  61.3 11.6 %all_to_all.23 = bf16[32,4,128]{2,1,0:T(4,128)(2,1)S(1)} all-to-all(bf16[32,4,128]{2,1,0:T(4,128)(2,1)S(1)} %bitcast.15), channel_id=1, replica_groups=mesh['z'=8,'x'=4,'y'=8,'c'=2] {'z','x'}, dimensions={0} | all-to-all | bytes 65536 | tf_op jit(solution)/shard_map/all_to_all | solution.py:305
  72.9 0.8 %shard_map.96 = bf16[8,128]{1,0:T(8,128)(2,1)} custom-call(bf16[128,128]{1,0:T(8,128)(2,1)S(1)} %bitcast.16, bf16[128,24]{1,0:T(8,128)(2,1)S(1)} %get-tuple-element.14.weights), custom_call_target="tpu_custom_call" | custom-call | tf_op jit(solution)/shard_map/pallas_call | solution.py:40
Async XLA Ops:
  0.0 23.3 %copy-start = (bf16[2,128,1024]{2,1,0:T(8,128)(2,1)S(1)}, bf16[2,128,1024]{2,1,0:T(8,128)(2,1)}, u32[]{:S(2)}) copy-start(bf16[2,128,1024]{2,1,0:T(8,128)(2,1)} %gate.3) | copy-start | bytes 1572868
  0.0 23.3 %copy-start.1 = (bf16[2,128,1024]{2,1,0:T(8,128)(2,1)S(1)}, bf16[2,128,1024]{2,1,0:T(8,128)(2,1)}, u32[]{:S(2)}) copy-start(bf16[2,128,1024]{2,1,0:T(8,128)(2,1)} %up.3) | copy-start | bytes 1572868
  46.0 14.9 %copy-start.2 = (bf16[2,1024,128]{2,1,0:T(8,128)(2,1)S(1)}, bf16[2,1024,128]{2,1,0:T(8,128)(2,1)}, u32[]{:S(2)}) copy-start(bf16[2,1024,128]{2,1,0:T(8,128)(2,1)} %down.1) | copy-start | bytes 1572868

commit v5 on v4

--- a/solution.py
+++ b/solution.py
@@ -102,15 +102,15 @@
     pair = jnp.concatenate([chosen, none], axis=1)
     slot_pair = jnp.concatenate([slots, none], axis=1)
     row = iota((place, 16), 0)
-    hit = (row // per == pair) & (row % (2 * SLOTS) == slot_pair)
+    hit = (row // per == pair) & (row % SLOTS == slot_pair)
     values = near_tokens[...].astype(f32)
     values = jnp.concatenate([values, jnp.zeros_like(values)], axis=0).astype(bf16)
     out[...] = dot(jnp.where(hit, 1.0, 0.0).astype(bf16), values).astype(bf16)
 
     likely = near_probs[...]
     shares = likely / jnp.sum(likely, axis=0, keepdims=True)
-    row = iota((place, 8), 0)
-    total = jnp.zeros((place, 8), f32)
+    row = iota((2 * place, 8), 0)
+    total = jnp.zeros((2 * place, 8), f32)
     for k in range(members.shape[0]):
         member = near_members[k : k + 1, :]
         at = (chosen * (EPG // 2) + member // 2) * (2 * SLOTS) + (member % 2) * SLOTS + slots
@@ -120,11 +120,8 @@
 
 
 def spread_body(core, arrived, affine, gate, up, kept, given):
-    places = arrived.shape[0]
-    rows = places // 2
-    at, source = iota((rows, places), 0), iota((rows, places), 1)
-    takes = source == (at // SLOTS) * (2 * SLOTS) + at % SLOTS
-    values = dot(jnp.where(takes, 1.0, 0.0).astype(bf16), arrived[...])
+    rows = arrived.shape[0]
+    values = arrived[...].astype(f32)
     mean = jnp.sum(values, axis=1, keepdims=True) / LANES
     centred = values - mean
     square = jnp.sum(centred * centred, axis=1, keepdims=True)
@@ -255,7 +252,7 @@
     at = core.reshape(1)
     outgoing, weights, affine = call(
         place_body,
-        (shape((places, LANES)), shape((places, 3 * count)), shape((8, LANES))),
+        (shape((rows, LANES)), shape((places, 3 * count)), shape((8, LANES))),
         [SMEM] + [ANY] * 8,
         scratch=[
             pltpu.VMEM(tokens.shape, tokens.dtype),
@@ -278,8 +275,8 @@
         up_weight,
     )
     arrived = lax.all_to_all(
-        outgoing.reshape(peers, 2 * SLOTS, LANES), ep, split_axis=0, concat_axis=0, tiled=True
-    ).reshape(places, LANES)
+        outgoing.reshape(peers, SLOTS, LANES), ep, split_axis=0, concat_axis=0, tiled=True
+    ).reshape(rows, LANES)
 
     whole = (tiles, rows + 8, 2 * LANES)
     kept, given = call(

time: 73.9 us -> 73.8 us (level)
  no operation moved by 1% of the time
where the time goes in v5:
time: 73.8 us; the launch traced here: 73.5 us
  blocking collectives  70.3 us (95%)
  Pallas kernels  3.16 us (4%)
    all_to_all x1, blocking collectives, on_device(): lax.all_to_all(outgoing.reshape(peers, SLOTS, LANES), ep, split_axis=0, c...  22.1 us
    all_to_all x1, blocking collectives, on_device(): parts = lax.all_to_all(parts, 'y', split_axis=0, concat_axis=0, tiled=True)  18 us
    all_to_all x1, blocking collectives, on_device(): lax.all_to_all(results.reshape(peers, 2 * SLOTS, LANES), ep, split_axis=0...  11.6 us
    all_to_all x1, blocking collectives, on_device(): lax.all_to_all(hidden, 'y', split_axis=0, concat_axis=0, tiled=True)  10.1 us
    all_gather x1, blocking collectives, on_device(): hidden = lax.all_gather(hidden, 'c', axis=0, tiled=False)  4.42 us
    all_gather x1, blocking collectives, on_device(): both = lax.all_gather(given, 'c', axis=0, tiled=False)  3.96 us
    pallas_call x6, Pallas kernels, run(): return kernel(*near)  3.16 us

profile of v5, /device:TPU:1, one launch (start us, length us, event | category | flops | bytes accessed | tf_op | source)
XLA Modules:
  0.0 73.5 jit_solution(8539258894727319006)
XLA Ops:
  0.0 0.0 copy-start
  0.0 0.0 copy-start.1
  0.0 1.1 %shard_map.91 = (bf16[64,128]{1,0:T(8,128)(2,1)S(1)}, bf16[128,24]{1,0:T(8,128)(2,1)S(1)}, bf16[8,128]{1,0:T(8,128)(2,1)S(1)}) custom-call(s32[1]{0:T(128)} %bitcast.core, bf16[8,128]{1,0:T(8,128)(2,1)} %tokens.1, s32[1,8]{1,0:T(1,128)} %bitcast.20, s32[4,8]{1,0:T(4,128)} %bitcast.18, f32[4,8]{1,0:T(4,128)} %bitcast.19, f32[1,128]{1,0:T(1,128)} %bitcast.21, ...), custom_call_target="tpu_custom_call" | custom-call | tf_op jit(solution)/shard_map/pallas_call | solution.py:40
  1.1 22.1 %all_to_all.20 = bf16[32,2,128]{2,1,0:T(2,128)(2,1)S(1)} all-to-all(bf16[32,2,128]{2,1,0:T(2,128)(2,1)S(1)} %bitcast.17), channel_id=1, replica_groups=mesh['z'=8,'x'=4,'y'=8,'c'=2] {'z','x'}, dimensions={0} | all-to-all | bytes 32768 | tf_op jit(solution)/shard_map/all_to_all | solution.py:277
  23.2 0.0 copy-done
  23.2 0.0 copy-done.1
  23.2 0.4 shard_map.92
  23.7 4.0 %all-gather = bf16[16,72,256]{2,1,0:T(8,128)(2,1)S(1)} all-gather(bf16[8,72,256]{2,1,0:T(8,128)(2,1)S(1)} %get-tuple-element.13), channel_id=2, replica_groups=mesh['z'=8,'x'=4,'y'=8,'c'=2] {'c'}, dimensions={0}, use_global_device_ids=true | all-gather | bytes 884736 | tf_op jit(solution)/shard_map/all_gather | solution.py:289
  27.6 0.2 shard_map.93
  27.9 18.0 %all_to_all.21.parts = bf16[8,72,256]{2,1,0:T(8,128)(2,1)S(1)} all-to-all(bf16[8,72,256]{2,1,0:T(8,128)(2,1)S(1)} %shard_map.93), channel_id=1, replica_groups=mesh['z'=8,'x'=4,'y'=8,'c'=2] {'y'}, dimensions={0} | all-to-all | bytes 589824 | tf_op jit(solution)/shard_map/all_to_all | solution.py:291
  45.9 0.0 copy-start.2
  45.9 0.3 shard_map.94
  46.2 10.1 %all_to_all.22 = bf16[8,64,128]{2,1,0:T(8,128)(2,1)S(1)} all-to-all(bf16[8,64,128]{2,1,0:T(8,128)(2,1)S(1)} %shard_map.94), channel_id=1, replica_groups=mesh['z'=8,'x'=4,'y'=8,'c'=2] {'y'}, dimensions={0} | all-to-all | bytes 262144 | tf_op jit(solution)/shard_map/all_to_all | solution.py:293
  56.4 4.4 %all-gather.1 = bf16[16,64,128]{2,1,0:T(8,128)(2,1)S(1)} all-gather(bf16[8,64,128]{2,1,0:T(8,128)(2,1)S(1)} %all_to_all.22), channel_id=3, replica_groups=mesh['z'=8,'x'=4,'y'=8,'c'=2] {'c'}, dimensions={0}, use_global_device_ids=true | all-gather | bytes 393216 | tf_op jit(solution)/shard_map/all_gather | solution.py:294
  60.8 0.0 copy-done.2
  60.8 0.4 shard_map.95
  61.2 11.6 %all_to_all.23 = bf16[32,4,128]{2,1,0:T(4,128)(2,1)S(1)} all-to-all(bf16[32,4,128]{2,1,0:T(4,128)(2,1)S(1)} %bitcast.14), channel_id=1, replica_groups=mesh['z'=8,'x'=4,'y'=8,'c'=2] {'z','x'}, dimensions={0} | all-to-all | bytes 65536 | tf_op jit(solution)/shard_map/all_to_all | solution.py:302
  72.8 0.8 %shard_map.96 = bf16[8,128]{1,0:T(8,128)(2,1)} custom-call(bf16[128,128]{1,0:T(8,128)(2,1)S(1)} %bitcast.15, bf16[128,24]{1,0:T(8,128)(2,1)S(1)} %get-tuple-element.14.weights), custom_call_target="tpu_custom_call" | custom-call | tf_op jit(solution)/shard_map/pallas_call | solution.py:40
Async XLA Ops:
  0.0 23.2 %copy-start = (bf16[2,128,1024]{2,1,0:T(8,128)(2,1)S(1)}, bf16[2,128,1024]{2,1,0:T(8,128)(2,1)}, u32[]{:S(2)}) copy-start(bf16[2,128,1024]{2,1,0:T(8,128)(2,1)} %gate.3) | copy-start | bytes 1572868
  0.0 23.2 %copy-start.1 = (bf16[2,128,1024]{2,1,0:T(8,128)(2,1)S(1)}, bf16[2,128,1024]{2,1,0:T(8,128)(2,1)}, u32[]{:S(2)}) copy-start(bf16[2,128,1024]{2,1,0:T(8,128)(2,1)} %up.3) | copy-start | bytes 1572868
  45.9 14.9 %copy-start.2 = (bf16[2,1024,128]{2,1,0:T(8,128)(2,1)S(1)}, bf16[2,1024,128]{2,1,0:T(8,128)(2,1)}, u32[]{:S(2)}) copy-start(bf16[2,1024,128]{2,1,0:T(8,128)(2,1)} %down.1) | copy-start | bytes 1572868

commit v6 on v5

--- a/solution.py
+++ b/solution.py
@@ -14,6 +14,10 @@
 EPG = 8
 SLOTS = 2
 LANES = 128
+SUMS_Y = [4, 3, 5, 2, 6, 1, 7, 0]
+ROWS_Y = [4, 3, 5, 2, 6, 1, 7, 0]
+OUT_Z, OUT_X = [4, 3, 5, 2, 6, 1, 7, 0], [2, 1, 3, 0]
+BACK_Z, BACK_X = [4, 3, 5, 2, 6, 1, 7, 0], [2, 1, 3, 0]
 NORM_EPSILON = 1e-05
 
 VMEM = pl.BlockSpec(memory_space=pltpu.VMEM)
@@ -55,6 +59,17 @@
 
 def iota(dims, axis):
     return lax.broadcasted_iota(jnp.int32, dims, axis)
+
+
+def place_in(order, values):
+    at = jnp.zeros_like(values)
+    for i, value in enumerate(order):
+        at = jnp.where(values == value, i, at)
+    return at
+
+
+def ends(order_z, order_x):
+    return [z * len(order_x) + x for z in order_z for x in order_x]
 
 
 def by_row(rows, width):
@@ -99,7 +114,7 @@
     chosen = near_groups[...]
     slots = slots_of(chosen)
     none = jnp.full((1, 8), -1, jnp.int32)
-    pair = jnp.concatenate([chosen, none], axis=1)
+    pair = jnp.concatenate([place_in(OUT_Z, chosen), none], axis=1)
     slot_pair = jnp.concatenate([slots, none], axis=1)
     row = iota((place, 16), 0)
     hit = (row // per == pair) & (row % SLOTS == slot_pair)
@@ -113,7 +128,7 @@
     total = jnp.zeros((2 * place, 8), f32)
     for k in range(members.shape[0]):
         member = near_members[k : k + 1, :]
-        at = (chosen * (EPG // 2) + member // 2) * (2 * SLOTS) + (member % 2) * SLOTS + slots
+        at = (place_in(BACK_Z, chosen) * (EPG // 2) + place_in(BACK_X, member // 2)) * (2 * SLOTS) + (member % 2) * SLOTS + slots
         total = total + jnp.where(row == at, shares[k : k + 1, :], 0.0)
     weights[...] = jnp.concatenate(three(total), axis=1).astype(bf16)
     affine[...] = by_row(three(near_gain[...]) + three(near_bias[...]), LANES).astype(bf16)
@@ -211,7 +226,7 @@
     row, source = iota((places, rows), 0), iota((places, rows), 1)
     total = jnp.zeros((places, LANES), f32)
     for e in range(experts):
-        wide = jnp.concatenate([hidden[e, y] for y in range(tiles)], axis=1)
+        wide = jnp.concatenate([hidden[e, ROWS_Y.index(y)] for y in SUMS_Y], axis=1)
         result = dot(wide, down[e]).astype(bf16)
         puts = row == (source // SLOTS) * (2 * SLOTS) + e * SLOTS + source % SLOTS
         total = total + dot(jnp.where(puts, 1.0, 0.0).astype(bf16), result)
@@ -238,7 +253,7 @@
     up_weight,
     down_weight,
 ):
-    ep = ("z", "x")
+    ep = "e"
     peers = lax.axis_size(ep)
     tiles = lax.axis_size("y")
     count, width = tokens.shape
@@ -275,7 +290,7 @@
         up_weight,
     )
     arrived = lax.all_to_all(
-        outgoing.reshape(peers, SLOTS, LANES), ep, split_axis=0, concat_axis=0, tiled=True
+        outgoing.reshape(peers, SLOTS, LANES), ep, split_axis=0, concat_axis=0, tiled=True, axis_index_groups=[ends(OUT_Z, OUT_X)]
     ).reshape(rows, LANES)
 
     whole = (tiles, rows + 8, 2 * LANES)
@@ -288,9 +303,13 @@
     )(at, arrived, affine, gate_weight, up_weight)
     both = lax.all_gather(given, "c", axis=0, tiled=False)
     parts = call(functools.partial(merge_body, width), shape(whole), [SMEM] + [VMEM] * 2)(at, kept, both)
-    parts = lax.all_to_all(parts, "y", split_axis=0, concat_axis=0, tiled=True)
+    parts = lax.all_to_all(
+        parts, "y", split_axis=0, concat_axis=0, tiled=True, axis_index_groups=[SUMS_Y]
+    )
     hidden = call(functools.partial(activate_body, features), shape((tiles, rows, LANES)), [VMEM])(parts)
-    hidden = lax.all_to_all(hidden, "y", split_axis=0, concat_axis=0, tiled=True)
+    hidden = lax.all_to_all(
+        hidden, "y", split_axis=0, concat_axis=0, tiled=True, axis_index_groups=[ROWS_Y]
+    )
     hidden = lax.all_gather(hidden, "c", axis=0, tiled=False)
     results = call(
         project_body,
@@ -300,14 +319,14 @@
         moved=down_weight.size * 2,
     )(hidden, down_weight)
     returned = lax.all_to_all(
-        results.reshape(peers, 2 * SLOTS, LANES), ep, split_axis=0, concat_axis=0, tiled=True
+        results.reshape(peers, 2 * SLOTS, LANES), ep, split_axis=0, concat_axis=0, tiled=True, axis_index_groups=[ends(BACK_Z, BACK_X)]
     ).reshape(places, LANES)
     return call(combine_body, jax.ShapeDtypeStruct((count, LANES), bf16), [VMEM] * 2)(returned, weights)
 
 
 def solution(mesh):
-    finer = Mesh(mesh.devices.reshape(8, 4, 8, 2), ("z", "x", "y", "c"))
-    ep, tp = ("z", "x"), ("y", "c")
+    finer = Mesh(mesh.devices.reshape(32, 8, 2), ("e", "y", "c"))
+    ep, tp = "e", ("y", "c")
     placed = (
         P(ep, tp),
         P(tp),

time: 73.8 us -> 67.2 us (0.911)
  blocking collectives: 70.3 us -> 63.7 us
    all_to_all x1, blocking collectives: 22.1 us -> 18.6 us  [on_device(): lax.all_to_all(outgoing.reshape(peers, SLOTS, LANES), ep, split_axis=0, c...]
    all_to_all x2, blocking collectives: 28.2 us -> 25.7 us  [the longest x1 15.7 us: on_device(): lax.all_to_all(parts, 'y', split_axis=0, concat_axis=0, tiled=True, axis_...]
    all_gather x1, blocking collectives: 4.42 us -> 3.45 us  [on_device(): hidden = lax.all_gather(hidden, 'c', axis=0, tiled=False)]
where the time goes in v6:
time: 67.2 us; the launch traced here: 66.9 us
  blocking collectives  63.7 us (95%)
  Pallas kernels  3.16 us (5%)
    all_to_all x1, blocking collectives, on_device(): lax.all_to_all(outgoing.reshape(peers, SLOTS, LANES), ep, split_axis=0, c...  18.6 us
    all_to_all x1, blocking collectives, on_device(): lax.all_to_all(parts, 'y', split_axis=0, concat_axis=0, tiled=True, axis_...  15.7 us
    all_to_all x1, blocking collectives, on_device(): lax.all_to_all(results.reshape(peers, 2 * SLOTS, LANES), ep, split_axis=0...  11.9 us
    all_to_all x1, blocking collectives, on_device(): lax.all_to_all(hidden, 'y', split_axis=0, concat_axis=0, tiled=True, axis...  9.94 us
    all_gather x1, blocking collectives, on_device(): both = lax.all_gather(given, 'c', axis=0, tiled=False)  3.96 us
    all_gather x1, blocking collectives, on_device(): hidden = lax.all_gather(hidden, 'c', axis=0, tiled=False)  3.45 us
    pallas_call x6, Pallas kernels, run(): return kernel(*near)  3.16 us

profile of v6, /device:TPU:1, one launch (start us, length us, event | category | flops | bytes accessed | tf_op | source)
XLA Modules:
  0.0 66.9 jit_solution(15080328829650857713)
XLA Ops:
  0.0 0.0 copy-start
  0.0 0.0 copy-start.1
  0.0 1.1 %shard_map.91 = (bf16[64,128]{1,0:T(8,128)(2,1)S(1)}, bf16[128,24]{1,0:T(8,128)(2,1)S(1)}, bf16[8,128]{1,0:T(8,128)(2,1)S(1)}) custom-call(s32[1]{0:T(128)} %bitcast.core, bf16[8,128]{1,0:T(8,128)(2,1)} %tokens.1, s32[1,8]{1,0:T(1,128)} %bitcast.20, s32[4,8]{1,0:T(4,128)} %bitcast.18, f32[4,8]{1,0:T(4,128)} %bitcast.19, f32[1,128]{1,0:T(1,128)} %bitcast.21, ...), custom_call_target="tpu_custom_call" | custom-call | tf_op jit(solution)/shard_map/pallas_call | solution.py:44
  1.1 18.6 %all_to_all.20 = bf16[32,2,128]{2,1,0:T(2,128)(2,1)S(1)} all-to-all(bf16[32,2,128]{2,1,0:T(2,128)(2,1)S(1)} %bitcast.17), channel_id=1, replica_groups={{288,272,304,256,224,208,240,192,352,336,368,320,160,144,176,128,416,40..., dimensions={0} | all-to-all | bytes 32768 | tf_op jit(solution)/shard_map/all_to_all | solution.py:292
  19.7 0.0 copy-done
  19.7 0.0 copy-done.1
  19.7 0.4 shard_map.92
  20.2 4.0 %all-gather = bf16[16,72,256]{2,1,0:T(8,128)(2,1)S(1)} all-gather(bf16[8,72,256]{2,1,0:T(8,128)(2,1)S(1)} %get-tuple-element.13), channel_id=2, replica_groups=mesh['e'=32,'y'=8,'c'=2] {'c'}, dimensions={0}, use_global_device_ids=true | all-gather | bytes 884736 | tf_op jit(solution)/shard_map/all_gather | solution.py:304
  24.1 0.2 shard_map.93
  24.4 15.7 %all_to_all.21.parts = bf16[8,72,256]{2,1,0:T(8,128)(2,1)S(1)} all-to-all(bf16[8,72,256]{2,1,0:T(8,128)(2,1)S(1)} %shard_map.93), channel_id=1, replica_groups={{8,6,10,4,12,2,14,0},{9,7,11,5,13,3,15,1},{24,22,26,20,28,18,30,16},{25..., dimensions={0} | all-to-all | bytes 589824 | tf_op jit(solution)/shard_map/all_to_all | solution.py:306
  40.1 0.0 copy-start.2
  40.1 0.3 shard_map.94
  40.4 9.9 %all_to_all.22 = bf16[8,64,128]{2,1,0:T(8,128)(2,1)S(1)} all-to-all(bf16[8,64,128]{2,1,0:T(8,128)(2,1)S(1)} %shard_map.94), channel_id=1, replica_groups={{8,6,10,4,12,2,14,0},{9,7,11,5,13,3,15,1},{24,22,26,20,28,18,30,16},{25..., dimensions={0} | all-to-all | bytes 262144 | tf_op jit(solution)/shard_map/all_to_all | solution.py:310
  50.4 3.5 %all-gather.1 = bf16[16,64,128]{2,1,0:T(8,128)(2,1)S(1)} all-gather(bf16[8,64,128]{2,1,0:T(8,128)(2,1)S(1)} %all_to_all.22), channel_id=3, replica_groups=mesh['e'=32,'y'=8,'c'=2] {'c'}, dimensions={0}, use_global_device_ids=true | all-gather | bytes 393216 | tf_op jit(solution)/shard_map/all_gather | solution.py:313
  53.8 0.0 copy-done.2
  53.8 0.4 shard_map.95
  54.2 11.9 %all_to_all.23 = bf16[32,4,128]{2,1,0:T(4,128)(2,1)S(1)} all-to-all(bf16[32,4,128]{2,1,0:T(4,128)(2,1)S(1)} %bitcast.14), channel_id=1, replica_groups={{288,272,304,256,224,208,240,192,352,336,368,320,160,144,176,128,416,40..., dimensions={0} | all-to-all | bytes 65536 | tf_op jit(solution)/shard_map/all_to_all | solution.py:321
  66.2 0.8 %shard_map.96 = bf16[8,128]{1,0:T(8,128)(2,1)} custom-call(bf16[128,128]{1,0:T(8,128)(2,1)S(1)} %bitcast.15, bf16[128,24]{1,0:T(8,128)(2,1)S(1)} %get-tuple-element.14.weights), custom_call_target="tpu_custom_call" | custom-call | tf_op jit(solution)/shard_map/pallas_call | solution.py:44
Async XLA Ops:
  0.0 19.7 %copy-start = (bf16[2,128,1024]{2,1,0:T(8,128)(2,1)S(1)}, bf16[2,128,1024]{2,1,0:T(8,128)(2,1)}, u32[]{:S(2)}) copy-start(bf16[2,128,1024]{2,1,0:T(8,128)(2,1)} %gate.3) | copy-start | bytes 1572868
  0.0 19.7 %copy-start.1 = (bf16[2,128,1024]{2,1,0:T(8,128)(2,1)S(1)}, bf16[2,128,1024]{2,1,0:T(8,128)(2,1)}, u32[]{:S(2)}) copy-start(bf16[2,128,1024]{2,1,0:T(8,128)(2,1)} %up.3) | copy-start | bytes 1572868
  40.1 13.7 %copy-start.2 = (bf16[2,1024,128]{2,1,0:T(8,128)(2,1)S(1)}, bf16[2,1024,128]{2,1,0:T(8,128)(2,1)}, u32[]{:S(2)}) copy-start(bf16[2,1024,128]{2,1,0:T(8,128)(2,1)} %down.1) | copy-start | bytes 1572868

commit v7 on v6

--- a/solution.py
+++ b/solution.py
@@ -223,14 +223,14 @@
 def project_body(hidden, down, out):
     experts, tiles, rows, width = hidden.shape
     places = out.shape[0]
-    row, source = iota((places, rows), 0), iota((places, rows), 1)
-    total = jnp.zeros((places, LANES), f32)
+    row, source = iota((places, places), 0), iota((places, places), 1)
+    results = []
     for e in range(experts):
         wide = jnp.concatenate([hidden[e, ROWS_Y.index(y)] for y in SUMS_Y], axis=1)
-        result = dot(wide, down[e]).astype(bf16)
-        puts = row == (source // SLOTS) * (2 * SLOTS) + e * SLOTS + source % SLOTS
-        total = total + dot(jnp.where(puts, 1.0, 0.0).astype(bf16), result)
-    out[...] = total.astype(bf16)
+        results.append(dot(wide, down[e]).astype(bf16))
+    expert, slot = source // rows, source % rows
+    puts = row == (slot // SLOTS) * (2 * SLOTS) + expert * SLOTS + slot % SLOTS
+    out[...] = dot(jnp.where(puts, 1.0, 0.0).astype(bf16), jnp.concatenate(results, axis=0)).astype(bf16)
 
 
 def combine_body(returned, weights, out):

time: 67.2 us -> 67.1 us (level)
  no operation moved by 1% of the time
where the time goes in v7:
time: 67.1 us; the launch traced here: 66.8 us
  blocking collectives  63.7 us (95%)
  Pallas kernels  3.12 us (5%)
    all_to_all x1, blocking collectives, on_device(): lax.all_to_all(outgoing.reshape(peers, SLOTS, LANES), ep, split_axis=0, c...  18.6 us
    all_to_all x1, blocking collectives, on_device(): lax.all_to_all(parts, 'y', split_axis=0, concat_axis=0, tiled=True, axis_...  15.7 us
    all_to_all x1, blocking collectives, on_device(): lax.all_to_all(results.reshape(peers, 2 * SLOTS, LANES), ep, split_axis=0...  11.9 us
    all_to_all x1, blocking collectives, on_device(): lax.all_to_all(hidden, 'y', split_axis=0, concat_axis=0, tiled=True, axis...  9.94 us
    all_gather x1, blocking collectives, on_device(): both = lax.all_gather(given, 'c', axis=0, tiled=False)  3.96 us
    all_gather x1, blocking collectives, on_device(): hidden = lax.all_gather(hidden, 'c', axis=0, tiled=False)  3.45 us
    pallas_call x6, Pallas kernels, run(): return kernel(*near)  3.12 us

profile of v7, /device:TPU:1, one launch (start us, length us, event | category | flops | bytes accessed | tf_op | source)
XLA Modules:
  0.0 66.8 jit_solution(2748948938995247143)
XLA Ops:
  0.0 0.0 copy-start
  0.0 0.0 copy-start.1
  0.0 1.1 %shard_map.91 = (bf16[64,128]{1,0:T(8,128)(2,1)S(1)}, bf16[128,24]{1,0:T(8,128)(2,1)S(1)}, bf16[8,128]{1,0:T(8,128)(2,1)S(1)}) custom-call(s32[1]{0:T(128)} %bitcast.core, bf16[8,128]{1,0:T(8,128)(2,1)} %tokens.1, s32[1,8]{1,0:T(1,128)} %bitcast.20, s32[4,8]{1,0:T(4,128)} %bitcast.18, f32[4,8]{1,0:T(4,128)} %bitcast.19, f32[1,128]{1,0:T(1,128)} %bitcast.21, ...), custom_call_target="tpu_custom_call" | custom-call | tf_op jit(solution)/shard_map/pallas_call | solution.py:44
  1.1 18.6 %all_to_all.20 = bf16[32,2,128]{2,1,0:T(2,128)(2,1)S(1)} all-to-all(bf16[32,2,128]{2,1,0:T(2,128)(2,1)S(1)} %bitcast.17), channel_id=1, replica_groups={{288,272,304,256,224,208,240,192,352,336,368,320,160,144,176,128,416,40..., dimensions={0} | all-to-all | bytes 32768 | tf_op jit(solution)/shard_map/all_to_all | solution.py:292
  19.7 0.0 copy-done
  19.7 0.0 copy-done.1
  19.7 0.4 shard_map.92
  20.2 4.0 %all-gather = bf16[16,72,256]{2,1,0:T(8,128)(2,1)S(1)} all-gather(bf16[8,72,256]{2,1,0:T(8,128)(2,1)S(1)} %get-tuple-element.13), channel_id=2, replica_groups=mesh['e'=32,'y'=8,'c'=2] {'c'}, dimensions={0}, use_global_device_ids=true | all-gather | bytes 884736 | tf_op jit(solution)/shard_map/all_gather | solution.py:304
  24.1 0.2 shard_map.93
  24.4 15.7 %all_to_all.21.parts = bf16[8,72,256]{2,1,0:T(8,128)(2,1)S(1)} all-to-all(bf16[8,72,256]{2,1,0:T(8,128)(2,1)S(1)} %shard_map.93), channel_id=1, replica_groups={{8,6,10,4,12,2,14,0},{9,7,11,5,13,3,15,1},{24,22,26,20,28,18,30,16},{25..., dimensions={0} | all-to-all | bytes 589824 | tf_op jit(solution)/shard_map/all_to_all | solution.py:306
  40.1 0.0 copy-start.2
  40.1 0.3 shard_map.94
  40.4 9.9 %all_to_all.22 = bf16[8,64,128]{2,1,0:T(8,128)(2,1)S(1)} all-to-all(bf16[8,64,128]{2,1,0:T(8,128)(2,1)S(1)} %shard_map.94), channel_id=1, replica_groups={{8,6,10,4,12,2,14,0},{9,7,11,5,13,3,15,1},{24,22,26,20,28,18,30,16},{25..., dimensions={0} | all-to-all | bytes 262144 | tf_op jit(solution)/shard_map/all_to_all | solution.py:310
  50.4 3.5 %all-gather.1 = bf16[16,64,128]{2,1,0:T(8,128)(2,1)S(1)} all-gather(bf16[8,64,128]{2,1,0:T(8,128)(2,1)S(1)} %all_to_all.22), channel_id=3, replica_groups=mesh['e'=32,'y'=8,'c'=2] {'c'}, dimensions={0}, use_global_device_ids=true | all-gather | bytes 393216 | tf_op jit(solution)/shard_map/all_gather | solution.py:313
  53.8 0.0 copy-done.2
  53.8 0.3 shard_map.95
  54.2 11.9 %all_to_all.23 = bf16[32,4,128]{2,1,0:T(4,128)(2,1)S(1)} all-to-all(bf16[32,4,128]{2,1,0:T(4,128)(2,1)S(1)} %bitcast.14), channel_id=1, replica_groups={{288,272,304,256,224,208,240,192,352,336,368,320,160,144,176,128,416,40..., dimensions={0} | all-to-all | bytes 65536 | tf_op jit(solution)/shard_map/all_to_all | solution.py:321
  66.1 0.8 %shard_map.96 = bf16[8,128]{1,0:T(8,128)(2,1)} custom-call(bf16[128,128]{1,0:T(8,128)(2,1)S(1)} %bitcast.15, bf16[128,24]{1,0:T(8,128)(2,1)S(1)} %get-tuple-element.14.weights), custom_call_target="tpu_custom_call" | custom-call | tf_op jit(solution)/shard_map/pallas_call | solution.py:44
Async XLA Ops:
  0.0 19.7 %copy-start = (bf16[2,128,1024]{2,1,0:T(8,128)(2,1)S(1)}, bf16[2,128,1024]{2,1,0:T(8,128)(2,1)}, u32[]{:S(2)}) copy-start(bf16[2,128,1024]{2,1,0:T(8,128)(2,1)} %gate.3) | copy-start | bytes 1572868
  0.0 19.7 %copy-start.1 = (bf16[2,128,1024]{2,1,0:T(8,128)(2,1)S(1)}, bf16[2,128,1024]{2,1,0:T(8,128)(2,1)}, u32[]{:S(2)}) copy-start(bf16[2,128,1024]{2,1,0:T(8,128)(2,1)} %up.3) | copy-start | bytes 1572868
  40.1 13.7 %copy-start.2 = (bf16[2,1024,128]{2,1,0:T(8,128)(2,1)S(1)}, bf16[2,1024,128]{2,1,0:T(8,128)(2,1)}, u32[]{:S(2)}) copy-start(bf16[2,1024,128]{2,1,0:T(8,128)(2,1)} %down.1) | copy-start | bytes 1572868

commit v8 on v6

--- a/solution.py
+++ b/solution.py
@@ -14,7 +14,7 @@
 EPG = 8
 SLOTS = 2
 LANES = 128
-SUMS_Y = [4, 3, 5, 2, 6, 1, 7, 0]
+SUMS_Y = [5, 3, 4, 2, 6, 1, 7, 0]
 ROWS_Y = [4, 3, 5, 2, 6, 1, 7, 0]
 OUT_Z, OUT_X = [4, 3, 5, 2, 6, 1, 7, 0], [2, 1, 3, 0]
 BACK_Z, BACK_X = [4, 3, 5, 2, 6, 1, 7, 0], [2, 1, 3, 0]

time: 67.2 us -> 66.9 us (level)
  no operation moved by 1% of the time
where the time goes in v8:
time: 66.9 us; the launch traced here: 66.7 us
  blocking collectives  63.4 us (95%)
  Pallas kernels  3.16 us (5%)
    all_to_all x1, blocking collectives, on_device(): lax.all_to_all(outgoing.reshape(peers, SLOTS, LANES), ep, split_axis=0, c...  18.6 us
    all_to_all x1, blocking collectives, on_device(): lax.all_to_all(parts, 'y', split_axis=0, concat_axis=0, tiled=True, axis_...  15.7 us
    all_to_all x1, blocking collectives, on_device(): lax.all_to_all(results.reshape(peers, 2 * SLOTS, LANES), ep, split_axis=0...  11.9 us
    all_to_all x1, blocking collectives, on_device(): lax.all_to_all(hidden, 'y', split_axis=0, concat_axis=0, tiled=True, axis...  9.73 us
    all_gather x1, blocking collectives, on_device(): both = lax.all_gather(given, 'c', axis=0, tiled=False)  3.96 us
    all_gather x1, blocking collectives, on_device(): hidden = lax.all_gather(hidden, 'c', axis=0, tiled=False)  3.45 us
    pallas_call x6, Pallas kernels, run(): return kernel(*near)  3.16 us

profile of v8, /device:TPU:1, one launch (start us, length us, event | category | flops | bytes accessed | tf_op | source)
XLA Modules:
  0.0 66.7 jit_solution(11986591430462642011)
XLA Ops:
  0.0 0.0 copy-start
  0.0 0.0 copy-start.1
  0.0 1.1 %shard_map.91 = (bf16[64,128]{1,0:T(8,128)(2,1)S(1)}, bf16[128,24]{1,0:T(8,128)(2,1)S(1)}, bf16[8,128]{1,0:T(8,128)(2,1)S(1)}) custom-call(s32[1]{0:T(128)} %bitcast.core, bf16[8,128]{1,0:T(8,128)(2,1)} %tokens.1, s32[1,8]{1,0:T(1,128)} %bitcast.20, s32[4,8]{1,0:T(4,128)} %bitcast.18, f32[4,8]{1,0:T(4,128)} %bitcast.19, f32[1,128]{1,0:T(1,128)} %bitcast.21, ...), custom_call_target="tpu_custom_call" | custom-call | tf_op jit(solution)/shard_map/pallas_call | solution.py:44
  1.1 18.6 %all_to_all.20 = bf16[32,2,128]{2,1,0:T(2,128)(2,1)S(1)} all-to-all(bf16[32,2,128]{2,1,0:T(2,128)(2,1)S(1)} %bitcast.17), channel_id=1, replica_groups={{288,272,304,256,224,208,240,192,352,336,368,320,160,144,176,128,416,40..., dimensions={0} | all-to-all | bytes 32768 | tf_op jit(solution)/shard_map/all_to_all | solution.py:292
  19.7 0.0 copy-done
  19.7 0.0 copy-done.1
  19.7 0.4 shard_map.92
  20.2 4.0 %all-gather = bf16[16,72,256]{2,1,0:T(8,128)(2,1)S(1)} all-gather(bf16[8,72,256]{2,1,0:T(8,128)(2,1)S(1)} %get-tuple-element.13), channel_id=2, replica_groups=mesh['e'=32,'y'=8,'c'=2] {'c'}, dimensions={0}, use_global_device_ids=true | all-gather | bytes 884736 | tf_op jit(solution)/shard_map/all_gather | solution.py:304
  24.1 0.2 shard_map.93
  24.4 15.7 %all_to_all.21.parts = bf16[8,72,256]{2,1,0:T(8,128)(2,1)S(1)} all-to-all(bf16[8,72,256]{2,1,0:T(8,128)(2,1)S(1)} %shard_map.93), channel_id=1, replica_groups={{10,6,8,4,12,2,14,0},{11,7,9,5,13,3,15,1},{26,22,24,20,28,18,30,16},{27..., dimensions={0} | all-to-all | bytes 589824 | tf_op jit(solution)/shard_map/all_to_all | solution.py:306
  40.1 0.0 copy-start.2
  40.1 0.3 shard_map.94
  40.4 9.7 %all_to_all.22 = bf16[8,64,128]{2,1,0:T(8,128)(2,1)S(1)} all-to-all(bf16[8,64,128]{2,1,0:T(8,128)(2,1)S(1)} %shard_map.94), channel_id=1, replica_groups={{8,6,10,4,12,2,14,0},{9,7,11,5,13,3,15,1},{24,22,26,20,28,18,30,16},{25..., dimensions={0} | all-to-all | bytes 262144 | tf_op jit(solution)/shard_map/all_to_all | solution.py:310
  50.1 3.5 %all-gather.1 = bf16[16,64,128]{2,1,0:T(8,128)(2,1)S(1)} all-gather(bf16[8,64,128]{2,1,0:T(8,128)(2,1)S(1)} %all_to_all.22), channel_id=3, replica_groups=mesh['e'=32,'y'=8,'c'=2] {'c'}, dimensions={0}, use_global_device_ids=true | all-gather | bytes 393216 | tf_op jit(solution)/shard_map/all_gather | solution.py:313
  53.6 0.0 copy-done.2
  53.6 0.4 shard_map.95
  54.0 11.9 %all_to_all.23 = bf16[32,4,128]{2,1,0:T(4,128)(2,1)S(1)} all-to-all(bf16[32,4,128]{2,1,0:T(4,128)(2,1)S(1)} %bitcast.14), channel_id=1, replica_groups={{288,272,304,256,224,208,240,192,352,336,368,320,160,144,176,128,416,40..., dimensions={0} | all-to-all | bytes 65536 | tf_op jit(solution)/shard_map/all_to_all | solution.py:321
  65.9 0.8 %shard_map.96 = bf16[8,128]{1,0:T(8,128)(2,1)} custom-call(bf16[128,128]{1,0:T(8,128)(2,1)S(1)} %bitcast.15, bf16[128,24]{1,0:T(8,128)(2,1)S(1)} %get-tuple-element.14.weights), custom_call_target="tpu_custom_call" | custom-call | tf_op jit(solution)/shard_map/pallas_call | solution.py:44
Async XLA Ops:
  0.0 19.7 %copy-start = (bf16[2,128,1024]{2,1,0:T(8,128)(2,1)S(1)}, bf16[2,128,1024]{2,1,0:T(8,128)(2,1)}, u32[]{:S(2)}) copy-start(bf16[2,128,1024]{2,1,0:T(8,128)(2,1)} %gate.3) | copy-start | bytes 1572868
  0.0 19.7 %copy-start.1 = (bf16[2,128,1024]{2,1,0:T(8,128)(2,1)S(1)}, bf16[2,128,1024]{2,1,0:T(8,128)(2,1)}, u32[]{:S(2)}) copy-start(bf16[2,128,1024]{2,1,0:T(8,128)(2,1)} %up.3) | copy-start | bytes 1572868
  40.1 13.5 %copy-start.2 = (bf16[2,1024,128]{2,1,0:T(8,128)(2,1)S(1)}, bf16[2,1024,128]{2,1,0:T(8,128)(2,1)}, u32[]{:S(2)}) copy-start(bf16[2,1024,128]{2,1,0:T(8,128)(2,1)} %down.1) | copy-start | bytes 1572868

commit v9 on v6

--- a/solution.py
+++ b/solution.py
@@ -130,7 +130,7 @@
         member = near_members[k : k + 1, :]
         at = (place_in(BACK_Z, chosen) * (EPG // 2) + place_in(BACK_X, member // 2)) * (2 * SLOTS) + (member % 2) * SLOTS + slots
         total = total + jnp.where(row == at, shares[k : k + 1, :], 0.0)
-    weights[...] = jnp.concatenate(three(total), axis=1).astype(bf16)
+    weights[...] = jnp.concatenate(three(total)[0:2], axis=1).astype(bf16)
     affine[...] = by_row(three(near_gain[...]) + three(near_bias[...]), LANES).astype(bf16)
 
 
@@ -238,7 +238,7 @@
     total = lax.dot_general(
         weights[...], returned[...], (((0,), (0,)), ((), ())), preferred_element_type=f32
     )
-    total = total[0:count] + total[count : 2 * count] + total[2 * count :]
+    total = total[0:count] + total[count:]
     out[...] = total.astype(bf16)
 
 
@@ -267,7 +267,7 @@
     at = core.reshape(1)
     outgoing, weights, affine = call(
         place_body,
-        (shape((rows, LANES)), shape((places, 3 * count)), shape((8, LANES))),
+        (shape((rows, LANES)), shape((places, 2 * count)), shape((8, LANES))),
         [SMEM] + [ANY] * 8,
         scratch=[
             pltpu.VMEM(tokens.shape, tokens.dtype),

time: 67.2 us -> 67.2 us (level)
  no operation moved by 1% of the time
where the time goes in v9:
time: 67.2 us; the launch traced here: 66.9 us
  blocking collectives  63.7 us (95%)
  Pallas kernels  3.16 us (5%)
    all_to_all x1, blocking collectives, on_device(): lax.all_to_all(outgoing.reshape(peers, SLOTS, LANES), ep, split_axis=0, c...  18.6 us
    all_to_all x1, blocking collectives, on_device(): lax.all_to_all(parts, 'y', split_axis=0, concat_axis=0, tiled=True, axis_...  15.7 us
    all_to_all x1, blocking collectives, on_device(): lax.all_to_all(results.reshape(peers, 2 * SLOTS, LANES), ep, split_axis=0...  11.9 us
    all_to_all x1, blocking collectives, on_device(): lax.all_to_all(hidden, 'y', split_axis=0, concat_axis=0, tiled=True, axis...  9.94 us
    all_gather x1, blocking collectives, on_device(): both = lax.all_gather(given, 'c', axis=0, tiled=False)  3.96 us
    all_gather x1, blocking collectives, on_device(): hidden = lax.all_gather(hidden, 'c', axis=0, tiled=False)  3.45 us
    pallas_call x6, Pallas kernels, run(): return kernel(*near)  3.16 us

profile of v9, /device:TPU:1, one launch (start us, length us, event | category | flops | bytes accessed | tf_op | source)
XLA Modules:
  0.0 66.9 jit_solution(5737914725383066341)
XLA Ops:
  0.0 0.0 copy-start
  0.0 0.0 copy-start.1
  0.0 1.1 %shard_map.91 = (bf16[64,128]{1,0:T(8,128)(2,1)S(1)}, bf16[128,16]{1,0:T(8,128)(2,1)S(1)}, bf16[8,128]{1,0:T(8,128)(2,1)S(1)}) custom-call(s32[1]{0:T(128)} %bitcast.core, bf16[8,128]{1,0:T(8,128)(2,1)} %tokens.1, s32[1,8]{1,0:T(1,128)} %bitcast.20, s32[4,8]{1,0:T(4,128)} %bitcast.18, f32[4,8]{1,0:T(4,128)} %bitcast.19, f32[1,128]{1,0:T(1,128)} %bitcast.21, ...), custom_call_target="tpu_custom_call" | custom-call | tf_op jit(solution)/shard_map/pallas_call | solution.py:44
  1.1 18.6 %all_to_all.20 = bf16[32,2,128]{2,1,0:T(2,128)(2,1)S(1)} all-to-all(bf16[32,2,128]{2,1,0:T(2,128)(2,1)S(1)} %bitcast.17), channel_id=1, replica_groups={{288,272,304,256,224,208,240,192,352,336,368,320,160,144,176,128,416,40..., dimensions={0} | all-to-all | bytes 32768 | tf_op jit(solution)/shard_map/all_to_all | solution.py:292
  19.7 0.0 copy-done
  19.7 0.0 copy-done.1
  19.7 0.4 shard_map.92
  20.2 4.0 %all-gather = bf16[16,72,256]{2,1,0:T(8,128)(2,1)S(1)} all-gather(bf16[8,72,256]{2,1,0:T(8,128)(2,1)S(1)} %get-tuple-element.13), channel_id=2, replica_groups=mesh['e'=32,'y'=8,'c'=2] {'c'}, dimensions={0}, use_global_device_ids=true | all-gather | bytes 884736 | tf_op jit(solution)/shard_map/all_gather | solution.py:304
  24.1 0.2 shard_map.93
  24.4 15.7 %all_to_all.21.parts = bf16[8,72,256]{2,1,0:T(8,128)(2,1)S(1)} all-to-all(bf16[8,72,256]{2,1,0:T(8,128)(2,1)S(1)} %shard_map.93), channel_id=1, replica_groups={{8,6,10,4,12,2,14,0},{9,7,11,5,13,3,15,1},{24,22,26,20,28,18,30,16},{25..., dimensions={0} | all-to-all | bytes 589824 | tf_op jit(solution)/shard_map/all_to_all | solution.py:306
  40.1 0.0 copy-start.2
  40.1 0.3 shard_map.94
  40.4 9.9 %all_to_all.22 = bf16[8,64,128]{2,1,0:T(8,128)(2,1)S(1)} all-to-all(bf16[8,64,128]{2,1,0:T(8,128)(2,1)S(1)} %shard_map.94), channel_id=1, replica_groups={{8,6,10,4,12,2,14,0},{9,7,11,5,13,3,15,1},{24,22,26,20,28,18,30,16},{25..., dimensions={0} | all-to-all | bytes 262144 | tf_op jit(solution)/shard_map/all_to_all | solution.py:310
  50.4 3.5 %all-gather.1 = bf16[16,64,128]{2,1,0:T(8,128)(2,1)S(1)} all-gather(bf16[8,64,128]{2,1,0:T(8,128)(2,1)S(1)} %all_to_all.22), channel_id=3, replica_groups=mesh['e'=32,'y'=8,'c'=2] {'c'}, dimensions={0}, use_global_device_ids=true | all-gather | bytes 393216 | tf_op jit(solution)/shard_map/all_gather | solution.py:313
  53.8 0.0 copy-done.2
  53.8 0.4 shard_map.95
  54.2 11.9 %all_to_all.23 = bf16[32,4,128]{2,1,0:T(4,128)(2,1)S(1)} all-to-all(bf16[32,4,128]{2,1,0:T(4,128)(2,1)S(1)} %bitcast.14), channel_id=1, replica_groups={{288,272,304,256,224,208,240,192,352,336,368,320,160,144,176,128,416,40..., dimensions={0} | all-to-all | bytes 65536 | tf_op jit(solution)/shard_map/all_to_all | solution.py:321
  66.1 0.7 %shard_map.96 = bf16[8,128]{1,0:T(8,128)(2,1)} custom-call(bf16[128,128]{1,0:T(8,128)(2,1)S(1)} %bitcast.15, bf16[128,16]{1,0:T(8,128)(2,1)S(1)} %get-tuple-element.14.weights), custom_call_target="tpu_custom_call" | custom-call | tf_op jit(solution)/shard_map/pallas_call | solution.py:44
Async XLA Ops:
  0.0 19.7 %copy-start = (bf16[2,128,1024]{2,1,0:T(8,128)(2,1)S(1)}, bf16[2,128,1024]{2,1,0:T(8,128)(2,1)}, u32[]{:S(2)}) copy-start(bf16[2,128,1024]{2,1,0:T(8,128)(2,1)} %gate.3) | copy-start | bytes 1572868
  0.0 19.7 %copy-start.1 = (bf16[2,128,1024]{2,1,0:T(8,128)(2,1)S(1)}, bf16[2,128,1024]{2,1,0:T(8,128)(2,1)}, u32[]{:S(2)}) copy-start(bf16[2,128,1024]{2,1,0:T(8,128)(2,1)} %up.3) | copy-start | bytes 1572868
  40.1 13.7 %copy-start.2 = (bf16[2,1024,128]{2,1,0:T(8,128)(2,1)S(1)}, bf16[2,1024,128]{2,1,0:T(8,128)(2,1)}, u32[]{:S(2)}) copy-start(bf16[2,1024,128]{2,1,0:T(8,128)(2,1)} %down.1) | copy-start | bytes 1572868
